TPU v7x, 256 devices: a whole 4x4x8 slice. The times are simulated.
256 devices in a mesh: ep: 64 (over z, x, core), tp: 4 (over y).
Axes of the slice: x: 4, y: 4, z: 8, core: 2. Of those that a mesh axis runs over, the one named last changes fastest.
Arguments:
- query_latent: bfloat16 [8192, 512], P('ep'), may hold values from -6 to 6
- key_latent: bfloat16 [8192, 256], P('ep'), may hold values from -6 to 6
- rope_key: bfloat16 [8192, 64], P('ep'), may hold values from -500 to 500
- query_gain: float32 [512], replicated, may hold values from 0.1 to 1.9
- key_gain: float32 [256], replicated, may hold values from 0.1 to 1.9
- w_query: bfloat16 [512, 1024], P(None, 'tp'), may hold values from -0.25 to 0.25
- w_query_rope: bfloat16 [512, 512], P(None, 'tp'), may hold values from -0.25 to 0.25
- w_key: bfloat16 [256, 1024], P(None, 'tp'), may hold values from -0.375 to 0.375
- w_value: bfloat16 [256, 1024], P(None, 'tp'), may hold values from -0.375 to 0.375
- w_out: bfloat16 [1024, 2048], P('tp'), may hold values from -1.796875 to 1.796875
- tokens_b: bfloat16 [32768, 2048], P('ep'), may hold values from -6 to 6
- ffn_gain: float32 [2048], replicated, may hold values from 0.1 to 1.9
- route_expert: int32 [32768, 2], P('ep'), may hold values from 0 to 63, as said below
- route_weight: float32 [32768, 2], P('ep'), may hold values from 0.2 to 1
- w_gate: bfloat16 [64, 2048, 1024], P('ep', None, 'tp'), may hold values from -0.125 to 0.125
- w_up: bfloat16 [64, 2048, 1024], P('ep', None, 'tp'), may hold values from -0.125 to 0.125
- w_down: bfloat16 [64, 1024, 2048], P('ep', 'tp'), may hold values from -0.1875 to 0.1875
Outputs:
- mixer_out: bfloat16 [8192, 2048], P(('ep', 'tp'))
- moe_out: bfloat16 [32768, 2048], P('ep', 'tp')
Inputs may be any that keep to these rules, and one draw needn't show every extreme that they name: `route_expert`: expert e belongs to group e // 16. A row's 2 experts differ and lie in one group. Among the rows of one device along ep, every group is named by exactly 128 rows and every expert is named exactly 16 times.
All inputs are finite; a program needn't handle non-finite values.
Results may differ from a plain program's by a relative error of at most 0.013.
The roundings to bfloat16 on the way count: a program that leaves them out, or rounds other values in their place, can miss the bound.
Values may be sent and summed in bfloat16 or wider, within the bound.
A program may use at most 64 MiB of HBM per device.

v0:
```python
import math

import jax
import jax.numpy as jnp
from jax import lax
from jax.sharding import PartitionSpec as P

NOPE = 128
ROPE = 64
VDIM = 128
GRID_W = 64
TOPK = 2


epsilon = 1e-06
rotary_base = 10000.0
neg_large = -1e30


def in_one_piece(arrays, axis, dim, along):
    ends, at = ([], 0)
    for a in arrays[:-1]:
        at += a.shape[along]
        ends.append(at)
    both = jnp.concatenate(arrays, axis=along)
    return tuple(jnp.split(lax.all_gather(both, axis, axis=dim, tiled=True), ends, axis=along))


def in_blocks(array, dim, size):
    before, after = (array.shape[:dim], array.shape[dim + 1 :])
    return jnp.moveaxis(array.reshape(*before, size, -1, *after), dim, 0)


def sum_at_owner(array, axis, dim):
    size = lax.axis_size(axis)
    blocks = lax.all_to_all(in_blocks(array, dim, size), axis, 0, 0, tiled=True)
    return jnp.sum(blocks.astype(jnp.float32), axis=0)


def rms_scale(values_in, gain):
    widened = values_in.astype(jnp.float32)
    normed = widened * lax.rsqrt(jnp.mean(widened * widened, axis=-1, keepdims=True) + epsilon)
    return (normed * gain).astype(jnp.bfloat16)


def rotary_tables(positions):
    half_width = ROPE // 2
    inverse = rotary_base ** (-jnp.arange(0, half_width, 2, dtype=jnp.float32) / half_width)
    grid_row = (positions // GRID_W).astype(jnp.float32)
    grid_col = (positions % GRID_W).astype(jnp.float32)
    angle = jnp.concatenate([grid_row[:, None] * inverse, grid_col[:, None] * inverse], axis=-1)
    return (jnp.cos(angle), jnp.sin(angle))


def rotate(values_in, cosine, sine):
    even_part = values_in[..., 0::2]
    odd_part = values_in[..., 1::2]
    turned = jnp.stack(
        [even_part * cosine - odd_part * sine, even_part * sine + odd_part * cosine], axis=-1
    )
    return turned.reshape(values_in.shape)


def fold_blocks(carry, members, step_fn):
    piece_rows = members[0].shape[0]
    block_rows = math.gcd(piece_rows, 1024)
    stacked = tuple(
        (
            member.reshape((piece_rows // block_rows, block_rows) + member.shape[1:])
            for member in members
        )
    )

    def scan_step(inner_carry, blocks):
        return (step_fn(inner_carry, blocks), None)

    result, unused = lax.scan(scan_step, carry, stacked)
    return result


def mixer_half(
    query_latent,
    key_latent,
    rope_key,
    query_gain,
    key_gain,
    w_query,
    w_query_rope,
    w_key,
    w_value,
    w_out,
):
    tok_rows = query_latent.shape[0]
    local_heads = w_query.shape[1] // NOPE
    positions = lax.axis_index("ep") * tok_rows + jnp.arange(tok_rows, dtype=jnp.int32)
    cosine, sine = rotary_tables(positions)
    query_normed = rms_scale(query_latent, query_gain)
    query_nope = jnp.dot(query_normed, w_query, preferred_element_type=jnp.float32).astype(
        jnp.bfloat16
    )
    query_nope = query_nope.reshape(tok_rows, local_heads, NOPE)
    query_rot = jnp.dot(query_normed, w_query_rope, preferred_element_type=jnp.float32)
    query_rot = rotate(
        query_rot.reshape(tok_rows, local_heads, ROPE), cosine[:, None, :], sine[:, None, :]
    )
    query_rot = query_rot.astype(jnp.bfloat16)
    key_rot = rotate(rope_key.astype(jnp.float32), cosine, sine).astype(jnp.bfloat16)
    score_scale = (NOPE + ROPE) ** (-0.5)

    def expand(latent_rows):
        latent_count = latent_rows.shape[0]
        key_normed = rms_scale(latent_rows, key_gain)
        key_nope = jnp.dot(key_normed, w_key, preferred_element_type=jnp.float32).astype(
            jnp.bfloat16
        )
        value_rows = jnp.dot(key_normed, w_value, preferred_element_type=jnp.float32).astype(
            jnp.bfloat16
        )
        return (
            key_nope.reshape(latent_count, local_heads, NOPE),
            value_rows.reshape(latent_count, local_heads, VDIM),
        )

    def attend_block(carry, key_nope, value_rows, key_turn):
        run_max, run_total, run_acc = carry
        scores = jnp.einsum(
            "qhd,khd->hqk", query_nope, key_nope, preferred_element_type=jnp.float32
        )
        scores = scores + jnp.einsum(
            "qhd,kd->hqk", query_rot, key_turn, preferred_element_type=jnp.float32
        )
        scores = scores * score_scale
        new_max = jnp.maximum(run_max, jnp.max(scores, axis=-1))
        correction = jnp.exp(run_max - new_max)
        weights = jnp.exp(scores - new_max[..., None])
        new_total = run_total * correction + jnp.sum(weights, axis=-1)
        added = jnp.einsum(
            "hqk,khd->qhd",
            weights.astype(jnp.bfloat16),
            value_rows,
            preferred_element_type=jnp.float32,
        )
        new_acc = run_acc * jnp.transpose(correction)[..., None] + added
        return (new_max, new_total, new_acc)

    def step_latent(carry, blocks):
        key_nope, value_rows = expand(blocks[0])
        return attend_block(carry, key_nope, value_rows, blocks[1])

    initial = (
        jnp.full((local_heads, tok_rows), neg_large, jnp.float32),
        jnp.zeros((local_heads, tok_rows), jnp.float32),
        jnp.zeros((tok_rows, local_heads, VDIM), jnp.float32),
    )
    final = fold_blocks(initial, in_one_piece((key_latent, key_rot), "ep", 0, 1), step_latent)
    run_max, run_total, run_acc = final
    heads_out = (run_acc / jnp.transpose(run_total)[..., None]).astype(jnp.bfloat16)
    heads_out = heads_out.reshape(tok_rows, local_heads * VDIM)
    summed = sum_at_owner(
        jnp.dot(heads_out, w_out, preferred_element_type=jnp.float32).astype(jnp.bfloat16), "tp", 0
    )
    return summed.astype(jnp.bfloat16)


def expert_half(tokens_b, ffn_gain, route_expert, route_weight, w_gate, w_up, w_down):
    tok_rows = tokens_b.shape[0]
    expert_count = lax.axis_size("ep")
    capacity = TOPK * tok_rows // expert_count
    normed = rms_scale(tokens_b, ffn_gain)
    copies = route_expert.reshape(tok_rows * TOPK)
    chosen = (copies[:, None] == jnp.arange(expert_count, dtype=jnp.int32)[None, :]).astype(
        jnp.int32
    )
    earlier = jnp.cumsum(chosen, axis=0) - chosen
    slot_index = jnp.sum(earlier * chosen, axis=1)
    target = copies * capacity + slot_index
    source_row = (
        jnp.zeros((expert_count * capacity,), jnp.int32)
        .at[target]
        .set(jnp.arange(tok_rows * TOPK, dtype=jnp.int32) // TOPK)
    )
    outgoing = jnp.take(normed, source_row, axis=0)
    arrived = lax.all_to_all(outgoing, "ep", split_axis=0, concat_axis=0, tiled=True)
    gate_act = jnp.dot(arrived, w_gate[0], preferred_element_type=jnp.float32)
    up_act = jnp.dot(arrived, w_up[0], preferred_element_type=jnp.float32)
    hidden = (jax.nn.silu(gate_act) * up_act).astype(jnp.bfloat16)
    partial_term = jnp.dot(hidden, w_down[0], preferred_element_type=jnp.float32)
    shared = lax.psum_scatter(
        partial_term.astype(jnp.bfloat16), "tp", scatter_dimension=1, tiled=True
    )
    returned = lax.all_to_all(shared, "ep", split_axis=0, concat_axis=0, tiled=True)
    picked = (
        jnp.take(returned, target, axis=0)
        .astype(jnp.float32)
        .reshape(tok_rows, TOPK, returned.shape[1])
    )
    combined = jnp.sum(picked * route_weight[:, :, None], axis=1)
    return combined.astype(jnp.bfloat16)


def body(
    query_latent,
    key_latent,
    rope_key,
    query_gain,
    key_gain,
    w_query,
    w_query_rope,
    w_key,
    w_value,
    w_out,
    tokens_b,
    ffn_gain,
    route_expert,
    route_weight,
    w_gate,
    w_up,
    w_down,
):
    mixer_out = mixer_half(
        query_latent,
        key_latent,
        rope_key,
        query_gain,
        key_gain,
        w_query,
        w_query_rope,
        w_key,
        w_value,
        w_out,
    )
    moe_out = expert_half(tokens_b, ffn_gain, route_expert, route_weight, w_gate, w_up, w_down)
    return (mixer_out, moe_out)


def solution(mesh):
    in_specs = (
        P("ep", None),
        P("ep", None),
        P("ep", None),
        P(),
        P(),
        P(None, "tp"),
        P(None, "tp"),
        P(None, "tp"),
        P(None, "tp"),
        P("tp", None),
        P("ep", None),
        P(),
        P("ep", None),
        P("ep", None),
        P("ep", None, "tp"),
        P("ep", None, "tp"),
        P("ep", "tp", None),
    )
    out_specs = (P(("ep", "tp"), None), P("ep", "tp"))
    return jax.shard_map(body, mesh=mesh, in_specs=in_specs, out_specs=out_specs, check_vma=False)
```

profile of v0, /device:TPU:1, one launch (start us, length us, event | category | flops | bytes accessed | tf_op | source)
XLA Modules:
  0.0 321.5 jit_solution(16313920895755321430)
XLA Ops:
  14.2 31.1 %reduce-window.6 = s32[64,8,128]{2,1,0:T(8,128)S(1)} reduce-window(s32[64,8,128]{2,1,0:T(8,128)} %fusion.42, s32[]{:T(128)} %constant.109.clone.1), window={size=1x1x128 pad=0_0x0_0x127_0}, to_apply=%region_7.8 | reduce-window | flops 8323072 | bytes 524292 | tf_op jit(solution)/shard_map/reduce-window
  50.1 4.3 %scatter_custom_fusion = s32[1024]{0:T(1024)S(1)} fusion(s32[1024]{0:T(1024)S(1)} %bitcast.143, s32[1024]{0:T(1024)S(1)} %add_select_fusion, s32[]{:T(128)} %constant.109.clone.1), kind=kCustom, calls=%fused_computation.104 | custom fusion | bytes 4100 | tf_op jit(solution)/shard_map/scatter | solution.py:180
  54.4 2.1 fusion.22
  56.6 6.1 %gather_fusion = bf16[1024,2048]{1,0:T(8,128)(2,1)} fusion(bf16[512,2048]{1,0:T(8,128)(2,1)S(1)} %fusion.22, s32[1024]{0:T(1024)S(1)} %fusion.55), kind=kCustom, calls=%fused_computation | custom fusion | bytes 8392704 | tf_op jit(solution)/shard_map/jit(_take)/gather | solution.py:182
  62.7 4.7 %broadcast_select_fusion.1 = bf16[64,16,2048]{2,1,0:T(8,128)(2,1)} fusion(bf16[64,16,2048]{2,1,0:T(8,128)(2,1)} %bitcast.126, pred[64,16]{1,0:T(8,128)(4,1)S(1)} %broadcast_in_dim.55), kind=kLoop, calls=%fused_computation.38 | loop fusion | flops 2097152 | bytes 8389632 | tf_op jit(solution)/shard_map/jit(_take)/select_n | solution.py:182
  67.4 13.4 %all-to-all-start.1 = ((bf16[64,16,2048]{2,1,0:T(8,128)(2,1)}), bf16[64,16,2048]{2,1,0:T(8,128)(2,1)}, u32[]{:S(2)}, u32[]{:S(2)}) async-start(bf16[64,16,2048]{2,1,0:T(8,128)(2,1)} %broadcast_select_fusion.1), calls=%async_computation.1 | async-start | bytes 8388608 | tf_op jit(solution)/shard_map/all_to_all | solution.py:183
  81.9 99.4 %all-to-all-done.1 = bf16[64,16,2048]{2,1,0:T(8,128)(2,1)} async-done(((bf16[64,16,2048]{2,1,0:T(8,128)(2,1)}), bf16[64,16,2048]{2,1,0:T(8,128)(2,1)}, u32[]{:S(2)}, u32[]{:S(2)}) %all-to-all-start.1) | async-done | bytes 4194336 | tf_op jit(solution)/shard_map/all_to_all | solution.py:183
  181.3 4.4 %fusion.28 = f32[1024,256]{1,0:T(8,128)} fusion(bf16[1024,2048]{1,0:T(8,128)(2,1)} %bitcast.17, bf16[1,2048,256]{2,1,0:T(8,128)(2,1)S(1)} %copy-done.10), kind=kOutput, calls=%fused_computation.49 | convolution fusion | flops 1073741824 | bytes 6291456 | tf_op jit(solution)/shard_map/dot_general | solution.py:184
  185.7 9.2 %convolution_convert_fusion.2 = bf16[1024,2048]{1,0:T(8,128)(2,1)} fusion(bf16[1024,2048]{1,0:T(8,128)(2,1)} %bitcast.17, bf16[1,256,2048]{2,1,0:T(8,128)(2,1)S(1)} %copy-done, bf16[1,2048,256]{2,1,0:T(8,128)(2,1)} %param.34, f32[1024,256]{1,0:T(8,128)} %fusion.28), kind=kOutput, calls=%fused_computation.39 | convolution fusion | flops 2151153664 | bytes 11534336 | tf_op jit(solution)/shard_map/dot_general | solution.py:187
  195.0 1.6 slice-done
  196.6 1.6 copy.46
  198.2 4.5 %split.8 = bf16[8192,256]{1,0:T(8,128)(2,1)} slice(bf16[8192,320]{1,0:T(8,128)(2,1)} %all-gather.2.cloned.1.call-done), slice={[0:8192], [0:256]} | slice | bytes 8388608 | tf_op jit(solution)/shard_map/split | solution.py:26
  202.7 53.1 %while.15 = (s32[]{:T(128)}, f32[2,128]{1,0:T(2,128)S(1)}, f32[2,128]{1,0:T(2,128)S(1)}, f32[128,2,128]{0,2,1:T(8,128)S(1)}, bf16[8,1024,256]{2,1,0:T(8,128)(2,1...) while((s32[]{:T(128)}, f32[2,128]{1,0:T(2,128)S(1)}, ...), condition=%wide.region_5.6_spmd.clone, body=%wide.region_1.5_spmd.clone.sunk | while | flops 441551360 | bytes 9707149 | solution.py:77
  204.2 1.6 convolution_convert_fusion.7
  210.9 1.6 convolution_convert_fusion.7
  220.7 1.6 convolution_convert_fusion.8
  224.1 1.6 convolution_convert_fusion.7
  227.3 1.6 convolution_convert_fusion.8
  240.5 1.6 convolution_convert_fusion.8
  256.2 12.0 %all_to_all.26 = bf16[4,32,2048]{2,1,0:T(8,128)(2,1)S(1)} all-to-all(bf16[4,32,2048]{2,1,0:T(8,128)(2,1)S(1)} %bitcast.132), channel_id=1, replica_groups=mesh['ep'=64,'tp'=4] {'tp'}, dimensions={0} | all-to-all | bytes 1048576 | tf_op jit(solution)/shard_map/all_to_all | solution.py:36
  268.2 8.1 %all-to-all-start.2 = ((bf16[64,16,512]{2,1,0:T(8,128)(2,1)}), bf16[64,16,512]{2,1,0:T(8,128)(2,1)S(1)}, u32[]{:S(2)}, u32[]{:S(2)}) async-start(bf16[64,16,512]{2,1,0:T(8,128)(2,1)} %bitcast.134), calls=%async_computation.3 | async-start | bytes 2097152 | tf_op jit(solution)/shard_map/all_to_all | solution.py:191
  277.7 26.7 %all-to-all-done.2 = bf16[64,16,512]{2,1,0:T(8,128)(2,1)S(1)} async-done(((bf16[64,16,512]{2,1,0:T(8,128)(2,1)}), bf16[64,16,512]{2,1,0:T(8,128)(2,1)S(1)}, u32[]{:S(2)}, u32[]{:S(2)}) %all-to-all-start.2) | async-done | bytes 1048608 | tf_op jit(solution)/shard_map/all_to_all | solution.py:191
  304.5 4.0 %gather_fusion.1 = bf16[1024,512]{1,0:T(8,128)(2,1)S(1)} fusion(bf16[1024,512]{1,0:T(8,128)(2,1)S(1)} %bitcast.125, s32[1024]{0:T(1024)S(1)} %broadcast_clamp_fusion), kind=kCustom, calls=%fused_computation.1 | custom fusion | bytes 2101248 | tf_op jit(solution)/shard_map/jit(_take)/gather | solution.py:193
  308.9 5.2 %multiply_reduce_fusion = bf16[512,512]{1,0:T(8,128)(2,1)} fusion(bf16[512,2,512]{2,1,0:T(2,128)(2,1)S(1)} %gather.15, pred[512,2]{1,0:T(8,128)(4,1)S(1)} %copy.52, f32[512,2]{1,0:T(8,128)S(1)} %copy.54), kind=kLoop, calls=%fused_computation.41 | loop fusion | flops 1835008 | bytes 1577984 | tf_op jit(solution)/shard_map/reduce_sum | solution.py:197
  (167 shorter events, 57.1 us)
Async XLA Ops:
  8.0 177.8 %copy-start = (bf16[1,256,2048]{2,1,0:T(8,128)(2,1)S(1)}, bf16[1,256,2048]{2,1,0:T(8,128)(2,1)}, u32[]{:S(2)}) copy-start(bf16[1,256,2048]{2,1,0:T(8,128)(2,1)} %param.35) | copy-start | bytes 3145732
  8.0 40.5 %copy-start.1 = (bf16[512,2048]{1,0:T(8,128)(2,1)S(1)}, bf16[512,2048]{1,0:T(8,128)(2,1)}, u32[]{:S(2)}) copy-start(bf16[512,2048]{1,0:T(8,128)(2,1)} %param.29) | copy-start | bytes 6291460
  8.0 46.4 %copy-start.7 = (f32[2048]{0:T(1024)S(1)}, f32[2048]{0:T(1024)}, u32[]{:S(2)}) copy-start(f32[2048]{0:T(1024)} %param.30) | copy-start | bytes 24580
  8.0 186.9 %all-gather.2.cloned.1.call-start = ((), (), s32[]{:S(2)}) async-start(), calls=%async_computation.4 | async-start | bytes 6389760 | tf_op jit(solution)/shard_map/all_gather | solution.py:26
  67.4 13.7 %copy-start.2 = (bf16[128,512]{1,0:T(8,128)(2,1)S(1)}, bf16[128,512]{1,0:T(8,128)(2,1)}, u32[]{:S(2)}) copy-start(bf16[128,512]{1,0:T(8,128)(2,1)} %param.19) | copy-start | bytes 393220
  67.4 13.8 %copy-start.5 = (bf16[512,128]{1,0:T(8,128)(2,1)S(1)}, bf16[512,128]{1,0:T(8,128)(2,1)}, u32[]{:S(2)}) copy-start(bf16[512,128]{1,0:T(8,128)(2,1)} %param.25) | copy-start | bytes 393220
  67.4 13.8 %copy-start.8 = (f32[512]{0:T(512)S(1)}, f32[512]{0:T(512)}, u32[]{:S(2)}) copy-start(f32[512]{0:T(512)} %param.22) | copy-start | bytes 6148
  67.4 14.2 %copy-start.4 = (bf16[512,256]{1,0:T(8,128)(2,1)S(1)}, bf16[512,256]{1,0:T(8,128)(2,1)}, u32[]{:S(2)}) copy-start(bf16[512,256]{1,0:T(8,128)(2,1)} %param.24) | copy-start | bytes 786436
  67.4 113.9 %copy-start.10 = (bf16[1,2048,256]{2,1,0:T(8,128)(2,1)S(1)}, bf16[1,2048,256]{2,1,0:T(8,128)(2,1)}, u32[]{:S(2)}) copy-start(bf16[1,2048,256]{2,1,0:T(8,128)(2,1)} %param.33) | copy-start | bytes 3145732
  67.4 113.9 %all-to-all-start.1 = ((bf16[64,16,2048]{2,1,0:T(8,128)(2,1)}), bf16[64,16,2048]{2,1,0:T(8,128)(2,1)}, u32[]{:S(2)}, u32[]{:S(2)}) async-start(bf16[64,16,2048]{2,1,0:T(8,128)(2,1)} %broadcast_select_fusion.1), calls=%async_computation.1 | async-start | bytes 8388608 | tf_op jit(solution)/shard_map/all_to_all | solution.py:183
  80.8 187.4 %reduce-scatter.2.cloned.1.call-start = ((), (), s32[]{:S(2)}) async-start(), calls=%async_computation.5 | async-start | bytes 5242880 | tf_op jit(solution)/shard_map/reduce_scatter | solution.py:188
  195.0 1.6 slice-start
  198.2 4.6 %copy-start.11 = (f32[256]{0:T(256)S(1)}, f32[256]{0:T(256)}, u32[]{:S(2)}) copy-start(f32[256]{0:T(256)} %param.23) | copy-start | bytes 3076
  202.7 53.1 %copy-start.3 = (bf16[256,2048]{1,0:T(8,128)(2,1)S(1)}, bf16[256,2048]{1,0:T(8,128)(2,1)}, u32[]{:S(2)}) copy-start(bf16[256,2048]{1,0:T(8,128)(2,1)} %param.28) | copy-start | bytes 3145732
  255.8 20.8 %copy-start.6 = (s32[512,2]{0,1:T(2,128)S(1)}, s32[512,2]{0,1:T(2,128)}, u32[]{:S(2)}) copy-start(s32[512,2]{0,1:T(2,128)} %param.31) | copy-start | bytes 12292
  255.8 21.0 %copy-start.9 = (f32[512,2]{0,1:T(2,128)S(1)}, f32[512,2]{0,1:T(2,128)}, u32[]{:S(2)}) copy-start(f32[512,2]{0,1:T(2,128)} %param.32) | copy-start | bytes 12292
  268.2 36.3 %all-to-all-start.2 = ((bf16[64,16,512]{2,1,0:T(8,128)(2,1)}), bf16[64,16,512]{2,1,0:T(8,128)(2,1)S(1)}, u32[]{:S(2)}, u32[]{:S(2)}) async-start(bf16[64,16,512]{2,1,0:T(8,128)(2,1)} %bitcast.134), calls=%async_computation.3 | async-start | bytes 2097152 | tf_op jit(solution)/shard_map/all_to_all | solution.py:191
Sparse Core Ops, SparseCore 0:
  12.2 97.7 all-gather.1
Sparse Core Ops, SparseCore 1:
  195.0 46.3 reduce-scatter.1
where the time goes:
time: 324 us; the launch traced here: 322 us
  waiting for transfers between devices  126 us (39%)
  other arithmetic  61.4 us (19%)
  matrix products  55 us (17%)
  local copies, waits for them, and re-layouts  28.7 us (9%)
  starting transfers between devices  21.8 us (7%)
  between operations  15.9 us (5%)
  blocking collectives  12 us (4%)
    all_to_all x1, waiting for transfers between devices, expert_half(): lax.all_to_all(outgoing, 'ep', split_axis=0, concat_axis=0, tiled=True)  99.4 us
    another operation x3, other arithmetic  32 us
    all_to_all x1, waiting for transfers between devices, expert_half(): lax.all_to_all(shared, 'ep', split_axis=0, concat_axis=0, tiled=True)  26.7 us
    all_to_all x1, starting transfers between devices, expert_half(): lax.all_to_all(outgoing, 'ep', split_axis=0, concat_axis=0, tiled=True)  13.4 us
    dot_general x8, matrix products, expand(): jnp.dot(key_normed, w_key, preferred_element_type=jnp.float32)  12.5 us
    dot_general x8, matrix products, expand(): jnp.dot(key_normed, w_value, preferred_element_type=jnp.float32)  12.5 us
    all_to_all x1, blocking collectives, sum_at_owner(): blocks = lax.all_to_all(in_blocks(array, dim, size), axis, 0, 0, tiled=True)  12 us
    reduce_sum x10, other arithmetic, rms_scale(): jnp.mean(widened * widened, axis=-1, keepdims=True) + epsilon  10.9 us
  transfers between devices with their start and end apart: 4, of which 2 were waited for; matrix products, arithmetic and copies ran while one was open for 41% of the time, Pallas kernels for 0%

commit v1 on v0

v1 whole, which is shorter than its diff:
```python
import math

import jax
import jax.numpy as jnp
import numpy as np
from jax import lax
from jax.experimental import pallas as pl
from jax.experimental.pallas import tpu as pltpu
from jax.sharding import PartitionSpec as P

NOPE = 128
ROPE = 64
GRID_W = 64
epsilon = 1e-06
rotary_base = 10000.0
LOG2E = 1.4426950408889634
SCORE_SCALE = (NOPE + ROPE) ** (-0.5)

F32 = jnp.float32
BF16 = jnp.bfloat16
MESH = pl.DeviceIdType.MESH

N_EP = 64
N_TP = 4
PER_Z = 8
N_Z = 8
CAP = 16
COLS = 512
CHUNK = PER_Z * CAP
HALF = CHUNK // 2
VMEM_LIMIT = 60 * 1024 * 1024


def rotary_consts():
    inverse = np.float32(rotary_base) ** (-np.arange(0, 32, 2, dtype=np.float32) / np.float32(32))
    inverse = inverse.astype(np.float32)
    entry = np.arange(128) % ROPE
    pair = entry // 2
    row_lane = pair < 16
    freq = inverse[pair % 16]
    row_angle = (np.arange(128, dtype=np.float32)[:, None] * freq[None, :]).astype(np.float32)
    col_angle = (np.arange(64, dtype=np.float32)[:, None] * freq[None, :]).astype(np.float32)

    def both(angle, keep):
        wide = angle.astype(np.float64)
        return [np.where(keep, fn(wide), 0.0).astype(np.float32) for fn in (np.cos, np.sin)]

    row_cos, row_sin = both(row_angle, row_lane[None, :])
    col_cos, col_sin = both(col_angle, ~row_lane[None, :])
    rows = np.stack([row_cos.reshape(64, 2, 128), row_sin.reshape(64, 2, 128)], axis=1)
    rows = rows.reshape(64, 4, 128)
    cols = np.stack([col_cos, col_sin], axis=0)
    return rows, cols


def cos_sin(rows_ref, cols_ref, ep):
    rows = rows_ref[ep]
    cos = jnp.concatenate([rows[0:1] + cols_ref[0], rows[1:2] + cols_ref[0]], axis=0)
    sin = jnp.concatenate([rows[2:3] + cols_ref[1], rows[3:4] + cols_ref[1]], axis=0)
    return cos, sin


def turn(x, cos, sin):
    lane = lax.broadcasted_iota(jnp.int32, x.shape, 1)
    swapped = jnp.where(lane % 2 == 0, -pltpu.roll(x, 127, 1), pltpu.roll(x, 1, 1))
    return x * cos + swapped * sin


def rms(x, gain):
    wide = x.astype(F32)
    normed = wide * lax.rsqrt(jnp.mean(wide * wide, axis=-1, keepdims=True) + epsilon)
    return (normed * gain).astype(BF16)


def prep_kernel(
    tok_ref, gain_ref, route_ref, klat_ref, rope_ref, kgain_ref, rows_ref, cols_ref,
    out_ref, target_ref, lat_ref, normed_ref,
):
    ep = lax.axis_index("ep")
    tp = lax.axis_index("tp")
    lane0 = pl.multiple_of(tp * COLS, COLS)
    lat_ref[0:128, :] = rms(klat_ref[...], kgain_ref[...])
    cos, sin = cos_sin(rows_ref, cols_ref, ep)
    rope = rope_ref[...].astype(F32)
    rope = jnp.concatenate([rope, rope], axis=0).T
    turned = turn(rope, cos, sin)
    low = lax.broadcasted_iota(jnp.int32, (32, 128), 1) < ROPE
    left = jnp.where(low, turned[0:32], turned[32:64])
    right = jnp.where(low, turned[64:96], turned[96:128])
    lat_ref[128:160, :] = jnp.concatenate([left, right], axis=1).astype(BF16)

    @pl.loop(0, 8)
    def _(i):
        sel = pl.ds(pl.multiple_of(i * 64, 64), 64)
        wide = tok_ref[sel, :].astype(F32)
        scale = lax.rsqrt(jnp.mean(wide * wide, axis=-1, keepdims=True) + epsilon)
        part = tok_ref[sel, pl.ds(lane0, COLS)].astype(F32)
        normed_ref[sel, :] = (part * scale * gain_ref[:, pl.ds(lane0, COLS)]).astype(BF16)

    route = route_ref[...]
    first = route[0:1, :]
    second = route[1:2, :]
    ids = lax.broadcasted_iota(jnp.int32, (N_EP, 512), 0)
    hit0 = (ids == first).astype(F32)
    hit1 = (ids == second).astype(F32)
    before = lax.broadcasted_iota(jnp.int32, (512, 512), 0) < lax.broadcasted_iota(
        jnp.int32, (512, 512), 1
    )
    earlier = jnp.dot((hit0 + hit1).astype(BF16), before.astype(BF16), preferred_element_type=F32)
    slot0 = jnp.sum(hit0 * earlier, axis=0, keepdims=True).astype(jnp.int32)
    slot1 = jnp.sum(hit1 * earlier, axis=0, keepdims=True).astype(jnp.int32)
    target0 = first * CAP + slot0
    target1 = second * CAP + slot1
    target_ref[0:1, :] = target0
    target_ref[1:2, :] = target1

    @pl.loop(0, 4)
    def _(i):
        base = i * 256
        ids = lax.broadcasted_iota(jnp.int32, (256, 512), 0) + base
        pick = ((ids == target0) | (ids == target1)).astype(BF16)
        rows = jnp.dot(pick, normed_ref[...], preferred_element_type=F32).astype(BF16)
        out_ref[pl.ds(i * CAP, CAP)] = rows.reshape(CAP, CAP, COLS)


def chunk_offset(c):
    return (c % 2) * (4 + c // 2) + (1 - c % 2) * ((4 - c // 2) % 4)


def remote(src, dst, send, recv, where):
    return pltpu.make_async_remote_copy(
        src_ref=src, dst_ref=dst, send_sem=send, recv_sem=recv, device_id=where, device_id_type=MESH
    )


def expert_kernel(
    out_ref, wg_hbm, wu_hbm, wd_hbm, ret_ref,
    wg, wu, wd, arr, part, rs1p, rs1m, rdp, rdm, sp, sm, rsp, rsm, res, hid,
    wsem, send, ra2a, ry0p, ry0m, rfwp, rfwm, r1p, r1m, r2p, r2m, r3p, r3m, rret,
):
    ep = lax.axis_index("ep")
    tp = lax.axis_index("tp")
    z = ep // PER_Z
    xc = ep % PER_Z
    up = (tp + 1) % N_TP
    down = (tp + N_TP - 1) % N_TP
    across = (tp + 2) % N_TP

    barrier = pltpu.get_barrier_semaphore()

    @pl.loop(1, N_EP)
    def _(i):
        pl.semaphore_signal(
            barrier, inc=1, device_id={"ep": (ep + i) % N_EP}, device_id_type=MESH
        )

    pl.semaphore_signal(barrier, inc=1, device_id={"tp": up}, device_id_type=MESH)
    pl.semaphore_signal(barrier, inc=1, device_id={"tp": down}, device_id_type=MESH)
    loads = [
        pltpu.make_async_copy(src, dst, wsem.at[i])
        for i, (src, dst) in enumerate(((wg_hbm, wg), (wu_hbm, wu), (wd_hbm, wd)))
    ]
    for load in loads:
        load.start()
    arr[tp, pl.ds(ep, 1)] = out_ref[pl.ds(ep, 1)]
    pl.semaphore_wait(barrier, N_EP - 1 + 2)

    @pl.loop(0, N_Z)
    def _(c):
        far = ((z + chunk_offset(c)) % N_Z) * PER_Z

        def put(other):
            remote(
                out_ref.at[other], arr.at[tp, ep], send.at[0], ra2a.at[c], {"ep": other}
            ).start()

        @pl.when(c != 0)
        def _():
            put(far + xc)

        @pl.loop(1, PER_Z)
        def _(j):
            put(far + (xc + j) % PER_Z)

    for load in loads:
        load.wait()

    def y_copy(src, dst, send_at, recv, where):
        return remote(src, dst, send.at[send_at], recv, {"tp": where})

    def plane(c):
        return ((z + N_Z - chunk_offset(c)) % N_Z) * PER_Z

    def stage0(c):
        at = plane(c)
        whole = arr.at[tp, pl.ds(at, PER_Z)]
        less = arr.at[tp, pl.ds(0, PER_Z - 1)]

        @pl.when(c == 0)
        def _():
            remote(less, less, send.at[0], ra2a.at[c], {"tp": up}).wait_recv()

        @pl.when(c != 0)
        def _():
            remote(whole, whole, send.at[0], ra2a.at[c], {"tp": up}).wait_recv()

        y_copy(whole, whole, 1, ry0p.at[c], up).start()
        y_copy(whole, whole, 2, ry0m.at[c], down).start()

    def stage1(c):
        at = plane(c)
        below = arr.at[down, pl.ds(at, PER_Z)]
        above = arr.at[up, pl.ds(at, PER_Z)]
        y_copy(below, below, 1, ry0p.at[c], up).wait_recv()
        half = arr.at[down, pl.ds(at, PER_Z // 2)]
        y_copy(half, half, 3, rfwp.at[c], up).start()
        y_copy(above, above, 2, ry0m.at[c], down).wait_recv()
        half = arr.at[up, pl.ds(at + PER_Z // 2, PER_Z // 2)]
        y_copy(half, half, 4, rfwm.at[c], down).start()

    def stage2(c):
        at = plane(c)
        half = arr.at[across, pl.ds(at, PER_Z // 2)]
        y_copy(half, half, 3, rfwp.at[c], up).wait_recv()
        half = arr.at[across, pl.ds(at + PER_Z // 2, PER_Z // 2)]
        y_copy(half, half, 4, rfwm.at[c], down).wait_recv()
        gate = jnp.zeros((CHUNK, 256), F32)
        upper = jnp.zeros((CHUNK, 256), F32)
        for q in range(N_TP):
            rows = arr[q, pl.ds(at, PER_Z)].reshape(CHUNK, COLS)
            gate += jnp.dot(rows, wg[q * COLS : (q + 1) * COLS, :], preferred_element_type=F32)
            upper += jnp.dot(rows, wu[q * COLS : (q + 1) * COLS, :], preferred_element_type=F32)
        hid[...] = (gate / (1.0 + jnp.exp(-gate)) * upper).astype(BF16)
        for q in range(N_TP):
            part[c, q] = jnp.dot(
                hid[...], wd[:, q * COLS : (q + 1) * COLS], preferred_element_type=F32
            ).astype(BF16)
        y_copy(part.at[c, across, pl.ds(0, HALF)], rs1p.at[c], 5, r1p.at[c], up).start()
        y_copy(part.at[c, across, pl.ds(HALF, HALF)], rs1m.at[c], 6, r1m.at[c], down).start()
        y_copy(part.at[c, up, pl.ds(HALF, HALF)], rdp.at[c], 7, r2p.at[c], up).start()
        y_copy(part.at[c, down, pl.ds(0, HALF)], rdm.at[c], 8, r2m.at[c], down).start()

    def stage3(c):
        y_copy(rs1p.at[c], rs1p.at[c], 5, r1p.at[c], up).wait_recv()
        sp[c] = (rs1p[c].astype(F32) + part[c, up, 0:HALF].astype(F32)).astype(BF16)
        y_copy(sp.at[c], rsp.at[c], 9, r3p.at[c], up).start()
        y_copy(rs1m.at[c], rs1m.at[c], 6, r1m.at[c], down).wait_recv()
        sm[c] = (rs1m[c].astype(F32) + part[c, down, HALF:CHUNK].astype(F32)).astype(BF16)
        y_copy(sm.at[c], rsm.at[c], 10, r3m.at[c], down).start()

    def stage4(c):
        at = plane(c)
        y_copy(rdp.at[c], rdp.at[c], 7, r2p.at[c], up).wait_recv()
        y_copy(rdm.at[c], rdm.at[c], 8, r2m.at[c], down).wait_recv()
        y_copy(rsp.at[c], rsp.at[c], 9, r3p.at[c], up).wait_recv()
        y_copy(rsm.at[c], rsm.at[c], 10, r3m.at[c], down).wait_recv()
        top = part[c, tp, 0:HALF].astype(F32) + rsp[c].astype(F32) + rdm[c].astype(F32)
        low = part[c, tp, HALF:CHUNK].astype(F32) + rdp[c].astype(F32) + rsm[c].astype(F32)
        res[c, 0 : PER_Z // 2] = top.astype(BF16).reshape(PER_Z // 2, CAP, COLS)
        res[c, PER_Z // 2 : PER_Z] = low.astype(BF16).reshape(PER_Z // 2, CAP, COLS)

        def put(j):
            remote(
                res.at[c, j], ret_ref.at[ep], send.at[11], rret.at[c], {"ep": at + j}
            ).start()

        @pl.when(c != 0)
        def _():
            put(xc)

        @pl.when(c == 0)
        def _():
            ret_ref[pl.ds(ep, 1)] = res[c, pl.ds(xc, 1)]

        @pl.loop(1, PER_Z)
        def _(j):
            put((xc + j) % PER_Z)

    stages = (stage0, stage1, stage2, stage3, stage4)

    @pl.loop(0, N_Z + len(stages) - 1)
    def _(i):
        for lag, stage in enumerate(stages):

            @pl.when((i >= lag) & (i < N_Z + lag))
            def _(stage=stage, lag=lag):
                stage(i - lag)

    @pl.loop(0, N_Z)
    def _(c):
        far = ((z + chunk_offset(c)) % N_Z) * PER_Z
        whole = ret_ref.at[pl.ds(far, PER_Z)]
        less = ret_ref.at[pl.ds(0, PER_Z - 1)]

        @pl.when(c == 0)
        def _():
            remote(less, less, send.at[11], rret.at[c], {"tp": up}).wait_recv()

        @pl.when(c != 0)
        def _():
            remote(whole, whole, send.at[11], rret.at[c], {"tp": up}).wait_recv()

    def sent(ref, which):
        remote(ref, ref, send.at[which], ra2a.at[0], {"tp": up}).wait_send()

    sent(out_ref.at[pl.ds(0, N_EP - 1)], 0)
    sent(arr.at[0], 1)
    sent(arr.at[0], 2)
    sent(arr.at[0, pl.ds(0, N_EP // 2)], 3)
    sent(arr.at[0, pl.ds(0, N_EP // 2)], 4)
    for which in range(5, 11):
        sent(rs1p, which)
    sent(out_ref.at[pl.ds(0, N_EP - 1)], 11)


def combine_kernel(target_ref, weight_ref, ret_ref, out_ref):
    pad = jnp.zeros((124, 512), F32)
    both = jnp.concatenate([target_ref[...].astype(F32), weight_ref[...], pad], axis=0)
    turned = both.T
    for i in range(4):
        rows = turned[i * 128 : (i + 1) * 128]
        ids = lax.broadcasted_iota(jnp.int32, (128, 1024), 1)
        total = jnp.zeros((128, COLS), F32)
        for c in range(2):
            pick = (ids == rows[:, c : c + 1].astype(jnp.int32)).astype(BF16)
            got = jnp.dot(pick, ret_ref[...], preferred_element_type=F32)
            total = total + got * rows[:, 2 + c : 3 + c]
        out_ref[i * 128 : (i + 1) * 128, :] = total.astype(BF16)


def mixer_kernel(
    qlat_ref, qgain_ref, wq_ref, wqr_ref, wk_ref, wv_ref, wo_ref, rows_ref, cols_ref, lat_ref,
    out_ref, qrot, top, total, acc, mix, got, send, recv,
):
    ep = lax.axis_index("ep")
    tp = lax.axis_index("tp")
    barrier = pltpu.get_barrier_semaphore()
    for i in range(1, N_TP):
        pl.semaphore_signal(
            barrier, inc=1, device_id={"tp": (tp + i) % N_TP}, device_id_type=MESH
        )
    qn = rms(qlat_ref[...], qgain_ref[...])
    nope = jnp.dot(qn, wq_ref[...], preferred_element_type=F32).astype(BF16)
    absorbed = [
        lax.dot_general(
            nope[:, h * 128 : (h + 1) * 128],
            wk_ref[:, h * 128 : (h + 1) * 128],
            (((1,), (1,)), ((), ())),
            preferred_element_type=F32,
        ).astype(BF16)
        for h in range(2)
    ]
    query = jnp.concatenate(absorbed, axis=0)
    cos, sin = cos_sin(rows_ref, cols_ref, ep)
    rot = turn(jnp.dot(qn, wqr_ref[...], preferred_element_type=F32), cos, sin)
    low = lax.broadcasted_iota(jnp.int32, (128, 128), 1) < ROPE
    rolled = pltpu.roll(rot, ROPE, 1)
    first = jnp.concatenate([jnp.where(low, rot, 0.0), jnp.where(low, rolled, 0.0)], axis=0)
    second = jnp.concatenate([jnp.where(low, 0.0, rolled), jnp.where(low, 0.0, rot)], axis=0)
    first = first.astype(BF16)
    second = second.astype(BF16)
    none = jnp.zeros((256, 128), BF16)
    for g, pair in enumerate(((first, none), (second, none), (none, first), (none, second))):
        qrot[g] = jnp.concatenate(pair, axis=1)
    top[...] = jnp.full((256, 1), -1e30, F32)
    total[...] = jnp.zeros((256, 1), F32)
    acc[...] = jnp.zeros((256, 256), F32)

    @pl.loop(0, 8)
    def _(i):
        g = i // 2
        blocks = pl.ds((i % 2) * 32, 32)
        keys = lat_ref[blocks, pl.ds(pl.multiple_of(g * 32, 32), 32), :].reshape(1024, 256)
        turned = lat_ref[blocks, 128:160, :].reshape(1024, 256)
        dims = (((1,), (1,)), ((), ()))
        scores = lax.dot_general(query, keys, dims, preferred_element_type=F32)
        scores += lax.dot_general(qrot[g], turned, dims, preferred_element_type=F32)
        scores = scores * (SCORE_SCALE * LOG2E)
        new_top = jnp.maximum(top[...], jnp.max(scores, axis=1, keepdims=True))
        fade = jnp.exp2(top[...] - new_top)
        weights = jnp.exp2(scores - new_top)
        total[...] = total[...] * fade + jnp.sum(weights, axis=1, keepdims=True)
        acc[...] = acc[...] * fade + jnp.dot(
            weights.astype(BF16), keys, preferred_element_type=F32
        )
        top[...] = new_top

    mean = (acc[...] / total[...]).astype(BF16)
    heads = [
        jnp.dot(
            mean[h * 128 : (h + 1) * 128],
            wv_ref[:, h * 128 : (h + 1) * 128],
            preferred_element_type=F32,
        ).astype(BF16)
        for h in range(2)
    ]
    heads = jnp.concatenate(heads, axis=1)
    for q in range(4):
        cols = slice(q * 512, (q + 1) * 512)
        mix[:, :, cols] = (
            jnp.dot(heads, wo_ref[:, cols], preferred_element_type=F32)
            .astype(BF16)
            .reshape(N_TP, 32, 512)
        )
    pl.semaphore_wait(barrier, N_TP - 1)
    copies = []
    for i in range(1, N_TP):
        other = (tp + i) % N_TP
        copies.append(remote(mix.at[other], got.at[i], send.at[i], recv.at[i], {"tp": other}))
        copies[-1].start()
    sums = mix[tp].astype(F32)
    for i in range(1, N_TP):
        copies[i - 1].wait()
        sums = sums + got[i].astype(F32)
    out_ref[...] = sums.astype(BF16)


VM = pl.BlockSpec(memory_space=pltpu.VMEM)
ANY = pl.BlockSpec(memory_space=pl.ANY)


def struct(shape, dtype=BF16):
    return jax.ShapeDtypeStruct(shape, dtype)


def body(
    query_latent, key_latent, rope_key, query_gain, key_gain, w_query, w_query_rope, w_key,
    w_value, w_out, tokens_b, ffn_gain, route_expert, route_weight, w_gate, w_up, w_down,
):
    rows_np, cols_np = rotary_consts()
    rows = jnp.asarray(rows_np)
    cols = jnp.asarray(cols_np)
    dma = pltpu.SemaphoreType.DMA

    outgoing, target, lat = pl.pallas_call(
        prep_kernel,
        out_shape=(
            struct((N_EP, CAP, COLS)),
            struct((2, 512), jnp.int32),
            struct((160, 256)),
        ),
        in_specs=[VM] * 8,
        out_specs=(VM, VM, VM),
        scratch_shapes=[pltpu.VMEM((512, COLS), BF16)],
        compiler_params=pltpu.CompilerParams(vmem_limit_bytes=VMEM_LIMIT),
        name="prep",
    )(
        tokens_b, ffn_gain.reshape(1, -1), route_expert.T, key_latent, rope_key.T,
        key_gain.reshape(1, -1), rows, cols,
    )
    gathered = lax.all_gather(lat, "ep", axis=0, tiled=True).reshape(N_EP, 160, 256)

    half = (N_Z, HALF, COLS)
    returned = pl.pallas_call(
        expert_kernel,
        out_shape=struct((N_EP, CAP, COLS)),
        in_specs=[VM, ANY, ANY, ANY],
        out_specs=VM,
        scratch_shapes=[
            pltpu.VMEM((2048, 256), BF16),
            pltpu.VMEM((2048, 256), BF16),
            pltpu.VMEM((256, 2048), BF16),
            pltpu.VMEM((N_TP, N_EP, CAP, COLS), BF16),
            pltpu.VMEM((N_Z, N_TP, CHUNK, COLS), BF16),
        ]
        + [pltpu.VMEM(half, BF16)] * 8
        + [
            pltpu.VMEM((N_Z, PER_Z, CAP, COLS), BF16),
            pltpu.VMEM((CHUNK, 256), BF16),
            dma((3,)),
            dma((12,)),
        ]
        + [dma((N_Z,))] * 12,
        compiler_params=pltpu.CompilerParams(
            collective_id=0, has_side_effects=True, vmem_limit_bytes=VMEM_LIMIT
        ),
        cost_estimate=pl.CostEstimate(flops=80_000_000_000, bytes_accessed=8_000_000, transcendentals=0),
        name="experts",
    )(outgoing, w_gate[0], w_up[0], w_down[0])

    moe_out = pl.pallas_call(
        combine_kernel,
        out_shape=struct((512, COLS)),
        in_specs=[VM] * 3,
        out_specs=VM,
        compiler_params=pltpu.CompilerParams(vmem_limit_bytes=VMEM_LIMIT),
        name="combine",
    )(target, route_weight.T, returned.reshape(N_EP * CAP, COLS))

    mixer_out = pl.pallas_call(
        mixer_kernel,
        out_shape=struct((32, 2048)),
        in_specs=[VM] * 10,
        out_specs=VM,
        scratch_shapes=[
            pltpu.VMEM((4, 256, 256), BF16),
            pltpu.VMEM((256, 1), F32),
            pltpu.VMEM((256, 1), F32),
            pltpu.VMEM((256, 256), F32),
            pltpu.VMEM((N_TP, 32, 2048), BF16),
            pltpu.VMEM((N_TP, 32, 2048), BF16),
            dma((N_TP,)),
            dma((N_TP,)),
        ],
        compiler_params=pltpu.CompilerParams(
            collective_id=1, has_side_effects=True, vmem_limit_bytes=VMEM_LIMIT
        ),
        cost_estimate=pl.CostEstimate(flops=8_000_000_000, bytes_accessed=8_000_000, transcendentals=0),
        name="mixer",
    )(
        query_latent, query_gain.reshape(1, -1), w_query, w_query_rope, w_key, w_value, w_out,
        rows, cols, gathered,
    )
    return (mixer_out, moe_out)


def solution(mesh):
    in_specs = (
        P("ep", None),
        P("ep", None),
        P("ep", None),
        P(),
        P(),
        P(None, "tp"),
        P(None, "tp"),
        P(None, "tp"),
        P(None, "tp"),
        P("tp", None),
        P("ep", None),
        P(),
        P("ep", None),
        P("ep", None),
        P("ep", None, "tp"),
        P("ep", None, "tp"),
        P("ep", "tp", None),
    )
    out_specs = (P(("ep", "tp"), None), P("ep", "tp"))
    return jax.shard_map(body, mesh=mesh, in_specs=in_specs, out_specs=out_specs, check_vma=False)
```

time: 324 us -> 151 us (0.47)
  Pallas kernels: 0 us -> 135 us
  waiting for transfers between devices: 126 us -> 0.02 us
  other arithmetic: 61.4 us -> 0 us
  matrix products: 55 us -> 0 us
  local copies, waits for them, and re-layouts: 28.7 us -> 1.57 us
  starting transfers between devices: 21.8 us -> 0.04 us
  blocking collectives: 12 us -> 0 us
    pallas_call x0 -> x4, Pallas kernels: none -> 135 us  [the longest x1 103 us: body(): pl.pallas_call(expert_kernel, out_shape=struct((N_EP, CAP, COLS)), in_spe...]
    all_to_all x2 -> x0, waiting for transfers between devices: 126 us -> none  [the longest x1 99.4 us: expert_half(): lax.all_to_all(outgoing, 'ep', split_axis=0, concat_axis=0, tiled=True)]
    dot_general x45 -> x0, matrix products: 55 us -> none  [the longest x8 12.5 us: expand(): jnp.dot(key_normed, w_key, preferred_element_type=jnp.float32)]
    another operation x7 -> x0, other arithmetic: 32.1 us -> none
    all_to_all x2 -> x0, starting transfers between devices: 21.5 us -> none  [the longest x1 13.4 us: expert_half(): lax.all_to_all(outgoing, 'ep', split_axis=0, concat_axis=0, tiled=True)]
    reduce_sum x21 -> x0, other arithmetic: 19.1 us -> none  [the longest x10 10.9 us: rms_scale(): jnp.mean(widened * widened, axis=-1, keepdims=True) + epsilon]
    all_to_all x1 -> x0, blocking collectives: 12 us -> none  [sum_at_owner(): blocks = lax.all_to_all(in_blocks(array, dim, size), axis, 0, 0, tiled=True)]
    gather x3 -> x0, local copies, waits for them, and re-layouts: 10.5 us -> none  [the longest x1 6.07 us: expert_half(): outgoing = jnp.take(normed, source_row, axis=0)]
  transfers between devices with their start and end apart: 4 -> 1, of which waited for: 2 -> 0; matrix products, arithmetic and copies ran while one was open for 41% -> 0% of each run, Pallas kernels for 0% -> 71%
where the time goes in v1:
time: 151 us
  Pallas kernels  135 us (89%)
  between operations  14 us (9%)
  local copies, waits for them, and re-layouts  1.57 us (1%)
    pallas_call x1, Pallas kernels, body(): pl.pallas_call(expert_kernel, out_shape=struct((N_EP, CAP, COLS)), in_spe...  103 us
    pallas_call x1, Pallas kernels, body(): pl.pallas_call(mixer_kernel, out_shape=struct((32, 2048)), in_specs=[VM]...  23.2 us
    pallas_call x1, Pallas kernels, body(): pl.pallas_call(prep_kernel, out_shape=(struct((N_EP, CAP, COLS)), struct(...  5.55 us
    pallas_call x1, Pallas kernels, body(): pl.pallas_call(combine_kernel, out_shape=struct((512, COLS)), in_specs=[V...  3.5 us
  transfers between devices with their start and end apart: 1, of which 0 were waited for; matrix products, arithmetic and copies ran while one was open for 0% of the time, Pallas kernels for 71%

profile of v1, /device:TPU:1, one launch (start us, length us, event | category | flops | bytes accessed | tf_op | source)
XLA Modules:
  0.0 150.7 jit_solution(2675417766763835243)
XLA Ops:
  7.2 0.0 all-gather.2.cloned.1.call-start
  7.2 5.6 %prep.1 = (bf16[64,16,512]{2,1,0:T(8,128)(2,1)}, s32[2,512]{1,0:T(2,128)}, bf16[160,256]{1,0:T(8,128)(2,1)}) custom-call(bf16[512,2048]{1,0:T(8,128)(2,1)} %tok_ref.1, f32[1,2048]{1,0:T(1,128)} %bitcast.13, s32[2,512]{1,0:T(2,128)} %bitcast.14, bf16[128,256]{1,0:T(8,128)(2,1)} %klat_ref.1, bf16[64,128]{1,0:T(8,128)(2,1)} %bitcast.12, f32[1,256]{1,0:T(1,128)} %bitcast.16, ...), custom_call_target="tpu_custom_call" | custom-call | tf_op jit(solution)/shard_map/prep/pallas_call | solution.py:435
  12.8 0.0 all-gather.2.cloned.1.call-update
  12.8 102.8 %experts.1 = bf16[64,16,512]{2,1,0:T(8,128)(2,1)} custom-call(bf16[64,16,512]{2,1,0:T(8,128)(2,1)} %get-tuple-element.7.out_ref, bf16[2048,256]{1,0:T(8,128)(2,1)} %bitcast.18, bf16[2048,256]{1,0:T(8,128)(2,1)} %bitcast.19, bf16[256,2048]{1,0:T(8,128)(2,1)} %bitcast.20), custom_call_target="tpu_custom_call" | custom-call | flops 80000000000 | bytes 8000000 | tf_op jit(solution)/shard_map/experts/pallas_call | solution.py:454
  115.6 3.5 %combine.1 = bf16[512,512]{1,0:T(8,128)(2,1)} custom-call(s32[2,512]{1,0:T(2,128)} %get-tuple-element.6.target_ref, f32[2,512]{1,0:T(2,128)} %bitcast.15, bf16[1024,512]{1,0:T(8,128)(2,1)} %bitcast.11), custom_call_target="tpu_custom_call" | custom-call | tf_op jit(solution)/shard_map/combine/pallas_call | solution.py:481
  119.1 0.0 all-gather.2.cloned.1.call-done
  119.1 23.2 %mixer.1 = bf16[32,2048]{1,0:T(8,128)(2,1)} custom-call(bf16[128,512]{1,0:T(8,128)(2,1)} %qlat_ref.1, f32[1,512]{1,0:T(1,128)} %bitcast.21, bf16[512,256]{1,0:T(8,128)(2,1)} %wq_ref.1, bf16[512,128]{1,0:T(8,128)(2,1)} %wqr_ref.1, bf16[256,256]{1,0:T(8,128)(2,1)} %wk_ref.1, bf16[256,256]{1,0:T(8,128)(2,1)} %wv_ref.1, bf16[256,2048]{1,0:T(8,128)(2,1)} %wo_ref.1, ...), custom_call_target="tpu_custom_call" | custom-call | flops 8000000000 | bytes 8000000 | tf_op jit(solution)/shard_map/mixer/pallas_call | solution.py:490
  142.3 1.6 %copy.22 = bf16[32,2048]{1,0:T(8,128)(2,1)} copy(bf16[32,2048]{1,0:T(8,128)(2,1)} %mixer.1) | data formatting | bytes 262144
Async XLA Ops:
  7.2 111.9 %all-gather.2.cloned.1.call-start = ((), (), s32[]{:S(2)}) async-start(), calls=%async_computation | async-start | bytes 5324800 | tf_op jit(solution)/shard_map/all_gather | solution.py:451
Sparse Core Ops, SparseCore 0:
  12.9 95.8 all-gather.1

commit v2 on v1

v2 whole, which is shorter than its diff:
```python
import math

import jax
import jax.numpy as jnp
import numpy as np
from jax import lax
from jax.experimental import pallas as pl
from jax.experimental.pallas import tpu as pltpu
from jax.sharding import PartitionSpec as P

NOPE = 128
ROPE = 64
GRID_W = 64
epsilon = 1e-06
rotary_base = 10000.0
LOG2E = 1.4426950408889634
SCORE_SCALE = (NOPE + ROPE) ** (-0.5)

F32 = jnp.float32
BF16 = jnp.bfloat16
MESH = pl.DeviceIdType.MESH

N_EP = 64
N_TP = 4
PER_Z = 8
N_Z = 8
CAP = 16
COLS = 512
CHUNK = PER_Z * CAP
HALF = CHUNK // 2
VMEM_LIMIT = 60 * 1024 * 1024


def rotary_consts():
    inverse = np.float32(rotary_base) ** (-np.arange(0, 32, 2, dtype=np.float32) / np.float32(32))
    inverse = inverse.astype(np.float32)
    entry = np.arange(128) % ROPE
    pair = entry // 2
    row_lane = pair < 16
    freq = inverse[pair % 16]
    row_angle = (np.arange(128, dtype=np.float32)[:, None] * freq[None, :]).astype(np.float32)
    col_angle = (np.arange(64, dtype=np.float32)[:, None] * freq[None, :]).astype(np.float32)

    def both(angle, keep):
        wide = angle.astype(np.float64)
        return [np.where(keep, fn(wide), 0.0).astype(np.float32) for fn in (np.cos, np.sin)]

    row_cos, row_sin = both(row_angle, row_lane[None, :])
    col_cos, col_sin = both(col_angle, ~row_lane[None, :])
    rows = np.stack([row_cos.reshape(64, 2, 128), row_sin.reshape(64, 2, 128)], axis=1)
    rows = rows.reshape(64, 4, 128)
    cols = np.stack([col_cos, col_sin], axis=0)
    return rows, cols


def cos_sin(rows_ref, cols_ref, ep):
    rows = rows_ref[ep]
    cos = jnp.concatenate([rows[0:1] + cols_ref[0], rows[1:2] + cols_ref[0]], axis=0)
    sin = jnp.concatenate([rows[2:3] + cols_ref[1], rows[3:4] + cols_ref[1]], axis=0)
    return cos, sin


def turn(x, cos, sin):
    lane = lax.broadcasted_iota(jnp.int32, x.shape, 1)
    swapped = jnp.where(lane % 2 == 0, -pltpu.roll(x, 127, 1), pltpu.roll(x, 1, 1))
    return x * cos + swapped * sin


def rms(x, gain):
    wide = x.astype(F32)
    normed = wide * lax.rsqrt(jnp.mean(wide * wide, axis=-1, keepdims=True) + epsilon)
    return (normed * gain).astype(BF16)


NT = (((1,), (1,)), ((), ()))


def chunk_offset(c):
    return (c % 2) * (4 + c // 2) + (1 - c % 2) * ((4 - c // 2) % 4)


def remote(src, dst, send, recv, where):
    return pltpu.make_async_remote_copy(
        src_ref=src, dst_ref=dst, send_sem=send, recv_sem=recv, device_id=where, device_id_type=MESH
    )


def main_kernel(
    gain_ref, route_ref, klat_ref, rope_ref, kgain_ref, qlat_ref, qgain_ref, rows_ref, cols_ref,
    tok_hbm, wg_hbm, wu_hbm, wd_hbm, wq_hbm, wqr_hbm, wk_hbm, wv_hbm, wo_hbm,
    ret_ref, target_ref, mixed_ref,
    tok, wg, wu, wq, wqr, wk, wv, wo, wdq, relay_p, relay_m,
    normed, outg, arr, hid, res, lat, query, qrot, top, total, acc, mix, got,
    wsem, send, rwd, rmix, ra2a, ry0p, ry0m, rfwp, rfwm, rh0p, rh0m, rhfp, rhfm, rret, rlz, rlx, rld,
):
    ep = lax.axis_index("ep")
    tp = lax.axis_index("tp")
    z = ep // PER_Z
    xc = ep % PER_Z
    x = xc // 2
    core = xc % 2
    up = (tp + 1) % N_TP
    down = (tp + N_TP - 1) % N_TP
    across = (tp + 2) % N_TP

    barrier = pltpu.get_barrier_semaphore()

    @pl.loop(1, N_EP)
    def _(i):
        pl.semaphore_signal(
            barrier, inc=1, device_id={"ep": (ep + i) % N_EP}, device_id_type=MESH
        )

    for other in (up, down, across):
        pl.semaphore_signal(barrier, inc=1, device_id={"tp": other}, device_id_type=MESH)

    def columns(which):
        return pl.ds(pl.multiple_of(which * COLS, COLS), COLS)

    pairs = (
        (tok_hbm, tok), (wd_hbm.at[:, columns(tp)], wdq.at[tp]), (wg_hbm, wg), (wu_hbm, wu),
        (wq_hbm, wq), (wqr_hbm, wqr), (wk_hbm, wk), (wv_hbm, wv), (wo_hbm, wo),
    )
    loads = [pltpu.make_async_copy(src, dst, wsem.at[i]) for i, (src, dst) in enumerate(pairs)]
    for load in loads:
        load.start()

    cos, sin = cos_sin(rows_ref, cols_ref, ep)
    lat[core, z, x, 0:128, :] = rms(klat_ref[...], kgain_ref[...])
    rope = rope_ref[...].astype(F32)
    rope = jnp.concatenate([rope, rope], axis=0).T
    turned = turn(rope, cos, sin)
    low = lax.broadcasted_iota(jnp.int32, (32, 128), 1) < ROPE
    left = jnp.where(low, turned[0:32], turned[32:64])
    right = jnp.where(low, turned[64:96], turned[96:128])
    lat[core, z, x, 128:160, :] = jnp.concatenate([left, right], axis=1).astype(BF16)

    route = route_ref[...]
    first = route[0:1, :]
    second = route[1:2, :]
    ids = lax.broadcasted_iota(jnp.int32, (N_EP, 512), 0)
    hit0 = (ids == first).astype(F32)
    hit1 = (ids == second).astype(F32)
    before = lax.broadcasted_iota(jnp.int32, (512, 512), 0) < lax.broadcasted_iota(
        jnp.int32, (512, 512), 1
    )
    earlier = jnp.dot((hit0 + hit1).astype(BF16), before.astype(BF16), preferred_element_type=F32)
    slot0 = jnp.sum(hit0 * earlier, axis=0, keepdims=True).astype(jnp.int32)
    slot1 = jnp.sum(hit1 * earlier, axis=0, keepdims=True).astype(jnp.int32)
    target_ref[0:1, :] = first * CAP + slot0
    target_ref[1:2, :] = second * CAP + slot1

    loads[0].wait()

    @pl.loop(0, 8)
    def _(i):
        sel = pl.ds(pl.multiple_of(i * 64, 64), 64)
        wide = tok[sel, :].astype(F32)
        scale = lax.rsqrt(jnp.mean(wide * wide, axis=-1, keepdims=True) + epsilon)
        part = tok[sel, columns(tp)].astype(F32)
        normed[sel, :] = (part * scale * gain_ref[:, columns(tp)]).astype(BF16)

    @pl.loop(0, 4)
    def _(i):
        ids = lax.broadcasted_iota(jnp.int32, (256, 512), 0) + i * 256
        pick = ((ids == target_ref[0:1, :]) | (ids == target_ref[1:2, :])).astype(BF16)
        rows = jnp.dot(pick, normed[...], preferred_element_type=F32).astype(BF16)
        outg[pl.ds(i * CAP, CAP)] = rows.reshape(CAP, CAP, COLS)

    arr[tp, pl.ds(ep, 1)] = outg[pl.ds(ep, 1)]
    pl.semaphore_wait(barrier, N_EP - 1 + 3)

    def y_copy(src, dst, send_at, recv, where):
        return remote(src, dst, send.at[send_at], recv, {"tp": where})

    y_copy(wd_hbm.at[:, columns(up)], wdq.at[tp], 0, rwd.at[0], up).start()
    y_copy(wd_hbm.at[:, columns(down)], wdq.at[tp], 1, rwd.at[1], down).start()
    y_copy(wd_hbm.at[pl.ds(0, 128), columns(across)], relay_p, 2, rwd.at[2], up).start()
    y_copy(wd_hbm.at[pl.ds(128, 128), columns(across)], relay_m, 3, rwd.at[3], down).start()

    @pl.loop(0, N_Z)
    def _(c):
        zd = (z + chunk_offset(c)) % N_Z
        far = zd * PER_Z

        def put(other):
            remote(outg.at[other], arr.at[tp, ep], send.at[6], ra2a.at[c], {"ep": other}).start()

        @pl.when(c != 0)
        def _():
            put(far + xc)

        @pl.loop(1, PER_Z)
        def _(j):
            put(far + (xc + j) % PER_Z)

        @pl.when(c != 0)
        def _():
            mine = lat.at[core, z, x]
            remote(mine, mine, send.at[7], rlz.at[c], {"ep": far + xc}).start()

    for load in loads[1:]:
        load.wait()

    qn = rms(qlat_ref[...], qgain_ref[...])
    nope = jnp.dot(qn, wq[...], preferred_element_type=F32).astype(BF16)
    for h in range(2):
        sel = slice(h * 128, (h + 1) * 128)
        query[sel, :] = lax.dot_general(
            nope[:, sel], wk[:, sel], NT, preferred_element_type=F32
        ).astype(BF16)
    rot = turn(jnp.dot(qn, wqr[...], preferred_element_type=F32), cos, sin)
    low = lax.broadcasted_iota(jnp.int32, (128, 128), 1) < ROPE
    rolled = pltpu.roll(rot, ROPE, 1)
    near = jnp.concatenate([jnp.where(low, rot, 0.0), jnp.where(low, rolled, 0.0)], axis=0)
    far = jnp.concatenate([jnp.where(low, 0.0, rolled), jnp.where(low, 0.0, rot)], axis=0)
    near = near.astype(BF16)
    far = far.astype(BF16)
    none = jnp.zeros((256, 128), BF16)
    for g, pair in enumerate(((near, none), (far, none), (none, near), (none, far))):
        qrot[g] = jnp.concatenate(pair, axis=1)
    top[...] = jnp.full((256, 1), -1e30, F32)
    total[...] = jnp.zeros((256, 1), F32)
    acc[...] = jnp.zeros((256, 256), F32)

    y_copy(relay_p, relay_p, 2, rwd.at[2], up).wait_recv()
    y_copy(relay_p, wdq.at[down, pl.ds(0, 128)], 4, rwd.at[4], up).start()
    y_copy(relay_m, relay_m, 3, rwd.at[3], down).wait_recv()
    y_copy(relay_m, wdq.at[up, pl.ds(128, 128)], 5, rwd.at[5], down).start()

    def plane(c):
        return (z + N_Z - chunk_offset(c)) % N_Z

    def tokens_in(c):
        at = plane(c) * PER_Z
        whole = arr.at[tp, pl.ds(at, PER_Z)]
        less = arr.at[tp, pl.ds(0, PER_Z - 1)]

        @pl.when(c == 0)
        def _():
            remote(less, less, send.at[6], ra2a.at[c], {"tp": up}).wait_recv()

        @pl.when(c != 0)
        def _():
            remote(whole, whole, send.at[6], ra2a.at[c], {"tp": up}).wait_recv()

        y_copy(whole, whole, 8, ry0p.at[c], up).start()
        y_copy(whole, whole, 9, ry0m.at[c], down).start()

    def tokens_on(c):
        at = plane(c) * PER_Z
        below = arr.at[down, pl.ds(at, PER_Z)]
        above = arr.at[up, pl.ds(at, PER_Z)]
        y_copy(below, below, 8, ry0p.at[c], up).wait_recv()
        half = arr.at[down, pl.ds(at, PER_Z // 2)]
        y_copy(half, half, 10, rfwp.at[c], up).start()
        y_copy(above, above, 9, ry0m.at[c], down).wait_recv()
        half = arr.at[up, pl.ds(at + PER_Z // 2, PER_Z // 2)]
        y_copy(half, half, 11, rfwm.at[c], down).start()

    def hidden_units(c):
        at = plane(c) * PER_Z
        half = arr.at[across, pl.ds(at, PER_Z // 2)]
        y_copy(half, half, 10, rfwp.at[c], up).wait_recv()
        half = arr.at[across, pl.ds(at + PER_Z // 2, PER_Z // 2)]
        y_copy(half, half, 11, rfwm.at[c], down).wait_recv()
        gate = jnp.zeros((CHUNK, 256), F32)
        upper = jnp.zeros((CHUNK, 256), F32)
        for q in range(N_TP):
            rows = arr[q, pl.ds(at, PER_Z)].reshape(CHUNK, COLS)
            gate += jnp.dot(rows, wg[q * COLS : (q + 1) * COLS, :], preferred_element_type=F32)
            upper += jnp.dot(rows, wu[q * COLS : (q + 1) * COLS, :], preferred_element_type=F32)
        hid[c, tp] = (gate / (1.0 + jnp.exp(-gate)) * upper).astype(BF16)
        mine = hid.at[c, tp]
        y_copy(mine, mine, 12, rh0p.at[c], up).start()
        y_copy(mine, mine, 13, rh0m.at[c], down).start()

    def hidden_on(c):
        y_copy(hid.at[c, down], hid.at[c, down], 12, rh0p.at[c], up).wait_recv()
        half = hid.at[c, down, pl.ds(0, HALF)]
        y_copy(half, half, 14, rhfp.at[c], up).start()
        y_copy(hid.at[c, up], hid.at[c, up], 13, rh0m.at[c], down).wait_recv()
        half = hid.at[c, up, pl.ds(HALF, HALF)]
        y_copy(half, half, 15, rhfm.at[c], down).start()

    def results_out(c):
        at = plane(c) * PER_Z

        @pl.when(c == 0)
        def _():
            whole = wdq.at[0]
            half = wdq.at[0, pl.ds(0, 128)]
            y_copy(whole, whole, 0, rwd.at[0], up).wait_recv()
            y_copy(whole, whole, 1, rwd.at[1], down).wait_recv()
            y_copy(half, half, 4, rwd.at[4], up).wait_recv()
            y_copy(half, half, 5, rwd.at[5], down).wait_recv()

        half = hid.at[c, across, pl.ds(0, HALF)]
        y_copy(half, half, 14, rhfp.at[c], up).wait_recv()
        half = hid.at[c, across, pl.ds(HALF, HALF)]
        y_copy(half, half, 15, rhfm.at[c], down).wait_recv()
        sums = jnp.zeros((CHUNK, COLS), F32)
        for q in range(N_TP):
            term = jnp.dot(hid[c, q], wdq[q], preferred_element_type=F32)
            sums += term.astype(BF16).astype(F32)
        res[c] = sums.astype(BF16).reshape(PER_Z, CAP, COLS)

        def put(j):
            remote(
                res.at[c, j], ret_ref.at[ep], send.at[16], rret.at[c], {"ep": at + j}
            ).start()

        @pl.when(c != 0)
        def _():
            put(xc)

        @pl.when(c == 0)
        def _():
            ret_ref[pl.ds(ep, 1)] = res[c, pl.ds(xc, 1)]

        @pl.loop(1, PER_Z)
        def _(j):
            put((xc + j) % PER_Z)

    def latents_x(c):
        block = lat.at[core, plane(c), x]

        @pl.when(c != 0)
        def _():
            remote(block, block, send.at[7], rlz.at[c], {"tp": up}).wait_recv()

        @pl.loop(1, 4)
        def _(j):
            there = z * PER_Z + ((x + j) % 4) * 2 + core
            remote(block, block, send.at[17], rlx.at[c], {"ep": there}).start()

    def latents_core(c):
        three = lat.at[core, 0, pl.ds(0, 3)]
        remote(three, three, send.at[17], rlx.at[c], {"tp": up}).wait_recv()
        four = lat.at[core, plane(c)]
        remote(four, four, send.at[18], rld.at[c], {"ep": z * PER_Z + x * 2 + (1 - core)}).start()

    def attend(c):
        at = plane(c)
        four = lat.at[1 - core, at]
        remote(four, four, send.at[18], rld.at[c], {"tp": up}).wait_recv()
        turned = lat[:, at, :, 128:160, :].reshape(256, 256)
        keys = []
        scores = []
        for g in range(4):
            keys.append(lat[:, at, :, g * 32 : (g + 1) * 32, :].reshape(256, 256))
            s = lax.dot_general(query[...], keys[g], NT, preferred_element_type=F32)
            s += lax.dot_general(qrot[g], turned, NT, preferred_element_type=F32)
            scores.append(s * (SCORE_SCALE * LOG2E))
        peak = jnp.maximum(
            jnp.maximum(scores[0], scores[1]), jnp.maximum(scores[2], scores[3])
        )
        new_top = jnp.maximum(top[...], jnp.max(peak, axis=1, keepdims=True))
        fade = jnp.exp2(top[...] - new_top)
        weighed = acc[...] * fade
        sums = jnp.zeros((256, 256), F32)
        for g in range(4):
            weights = jnp.exp2(scores[g] - new_top)
            sums += weights
            weighed += jnp.dot(weights.astype(BF16), keys[g], preferred_element_type=F32)
        total[...] = total[...] * fade + jnp.sum(sums, axis=1, keepdims=True)
        acc[...] = weighed
        top[...] = new_top

    def mix_copy(i):
        other = (tp + i) % N_TP
        return remote(mix.at[other], got.at[i], send.at[18 + i], rmix.at[i], {"tp": other})

    def project(c):
        mean = (acc[...] / total[...]).astype(BF16)
        heads = []
        for h in range(2):
            sel = slice(h * 128, (h + 1) * 128)
            heads.append(
                jnp.dot(mean[sel], wv[:, sel], preferred_element_type=F32).astype(BF16)
            )
        heads = jnp.concatenate(heads, axis=1)
        for q in range(4):
            sel = slice(q * 512, (q + 1) * 512)
            term = jnp.dot(heads, wo[:, sel], preferred_element_type=F32)
            mix[:, :, sel] = term.astype(BF16).reshape(N_TP, 32, 512)
        for i in range(1, N_TP):
            mix_copy(i).start()

    plan = (
        (0, N_Z, tokens_in),
        (0, N_Z, latents_x),
        (1, N_Z, tokens_on),
        (1, N_Z, latents_core),
        (2, N_Z, hidden_units),
        (2, N_Z, attend),
        (3, N_Z, hidden_on),
        (4, N_Z, results_out),
        (10, 1, project),
    )

    @pl.loop(0, 12)
    def _(i):
        for lag, count, stage in plan:

            @pl.when((i >= lag) & (i < lag + count))
            def _(stage=stage, lag=lag):
                stage(i - lag)

    sums = mix[tp].astype(F32)
    for i in range(1, N_TP):
        mix_copy(i).wait()
        sums = sums + got[i].astype(F32)
    mixed_ref[...] = sums.astype(BF16)

    @pl.loop(0, N_Z)
    def _(c):
        far = ((z + chunk_offset(c)) % N_Z) * PER_Z
        whole = ret_ref.at[pl.ds(far, PER_Z)]
        less = ret_ref.at[pl.ds(0, PER_Z - 1)]

        @pl.when(c == 0)
        def _():
            remote(less, less, send.at[16], rret.at[c], {"tp": up}).wait_recv()

        @pl.when(c != 0)
        def _():
            remote(whole, whole, send.at[16], rret.at[c], {"tp": up}).wait_recv()

    def sent(ref, which):
        remote(ref, ref, send.at[which], ra2a.at[0], {"tp": up}).wait_send()

    for which in (0, 1):
        sent(wdq.at[0], which)
    for which in (2, 3, 4, 5):
        sent(relay_p, which)
    sent(outg.at[pl.ds(0, N_EP - 1)], 6)
    sent(lat.at[0, pl.ds(0, 7), 0], 7)
    for which in (8, 9):
        sent(arr.at[0], which)
    for which in (10, 11):
        sent(arr.at[0, pl.ds(0, N_EP // 2)], which)
    for which in (12, 13):
        sent(hid.at[:, 0], which)
    for which in (14, 15):
        sent(hid.at[:, 0, pl.ds(0, HALF)], which)
    sent(outg.at[pl.ds(0, N_EP - 1)], 16)
    sent(lat.at[0, :, pl.ds(0, 3)], 17)
    sent(lat.at[0], 18)


def combine_kernel(target_ref, weight_ref, ret_ref, out_ref):
    pad = jnp.zeros((124, 512), F32)
    both = jnp.concatenate([target_ref[...].astype(F32), weight_ref[...], pad], axis=0)
    turned = both.T
    for i in range(4):
        rows = turned[i * 128 : (i + 1) * 128]
        ids = lax.broadcasted_iota(jnp.int32, (128, 1024), 1)
        total = jnp.zeros((128, COLS), F32)
        for c in range(2):
            pick = (ids == rows[:, c : c + 1].astype(jnp.int32)).astype(BF16)
            got = jnp.dot(pick, ret_ref[...], preferred_element_type=F32)
            total = total + got * rows[:, 2 + c : 3 + c]
        out_ref[i * 128 : (i + 1) * 128, :] = total.astype(BF16)


VM = pl.BlockSpec(memory_space=pltpu.VMEM)
ANY = pl.BlockSpec(memory_space=pl.ANY)


def struct(shape, dtype=BF16):
    return jax.ShapeDtypeStruct(shape, dtype)


def body(
    query_latent, key_latent, rope_key, query_gain, key_gain, w_query, w_query_rope, w_key,
    w_value, w_out, tokens_b, ffn_gain, route_expert, route_weight, w_gate, w_up, w_down,
):
    rows_np, cols_np = rotary_consts()
    rows = jnp.asarray(rows_np)
    cols = jnp.asarray(cols_np)
    dma = pltpu.SemaphoreType.DMA

    returned, target, mixer_out = pl.pallas_call(
        main_kernel,
        out_shape=(
            struct((N_EP, CAP, COLS)),
            struct((2, 512), jnp.int32),
            struct((32, 2048)),
        ),
        in_specs=[VM] * 9 + [ANY] * 9,
        out_specs=(VM, VM, VM),
        scratch_shapes=[
            pltpu.VMEM(shape, dtype)
            for shape, dtype in (
                ((512, 2048), BF16),
                ((2048, 256), BF16),
                ((2048, 256), BF16),
                ((512, 256), BF16),
                ((512, 128), BF16),
                ((256, 256), BF16),
                ((256, 256), BF16),
                ((256, 2048), BF16),
                ((N_TP, 256, COLS), BF16),
                ((128, COLS), BF16),
                ((128, COLS), BF16),
                ((512, COLS), BF16),
                ((N_EP, CAP, COLS), BF16),
                ((N_TP, N_EP, CAP, COLS), BF16),
                ((N_Z, N_TP, CHUNK, 256), BF16),
                ((N_Z, PER_Z, CAP, COLS), BF16),
                ((2, N_Z, 4, 160, 256), BF16),
                ((256, 256), BF16),
                ((4, 256, 256), BF16),
                ((256, 1), F32),
                ((256, 1), F32),
                ((256, 256), F32),
                ((N_TP, 32, 2048), BF16),
                ((N_TP, 32, 2048), BF16),
            )
        ]
        + [dma((9,)), dma((22,)), dma((6,)), dma((N_TP,))]
        + [dma((N_Z,))] * 13,
        compiler_params=pltpu.CompilerParams(
            collective_id=0, has_side_effects=True, vmem_limit_bytes=VMEM_LIMIT
        ),
        name="exchange",
    )(
        ffn_gain.reshape(1, -1), route_expert.T, key_latent, rope_key.T, key_gain.reshape(1, -1),
        query_latent, query_gain.reshape(1, -1), rows, cols,
        tokens_b, w_gate[0], w_up[0], w_down[0], w_query, w_query_rope, w_key, w_value, w_out,
    )

    moe_out = pl.pallas_call(
        combine_kernel,
        out_shape=struct((512, COLS)),
        in_specs=[VM] * 3,
        out_specs=VM,
        compiler_params=pltpu.CompilerParams(vmem_limit_bytes=VMEM_LIMIT),
        name="combine",
    )(target, route_weight.T, returned.reshape(N_EP * CAP, COLS))

    return (mixer_out, moe_out)


def solution(mesh):
    in_specs = (
        P("ep", None),
        P("ep", None),
        P("ep", None),
        P(),
        P(),
        P(None, "tp"),
        P(None, "tp"),
        P(None, "tp"),
        P(None, "tp"),
        P("tp", None),
        P("ep", None),
        P(),
        P("ep", None),
        P("ep", None),
        P("ep", None, "tp"),
        P("ep", None, "tp"),
        P("ep", "tp", None),
    )
    out_specs = (P(("ep", "tp"), None), P("ep", "tp"))
    return jax.shard_map(body, mesh=mesh, in_specs=in_specs, out_specs=out_specs, check_vma=False)
```

time: 151 us -> 103 us (0.68)
  Pallas kernels: 135 us -> 99.1 us
  between operations: 14 us -> 0.65 us
    pallas_call x3 -> x1, Pallas kernels: 132 us -> 95.6 us  [body(): pl.pallas_call(main_kernel, out_shape=(struct((N_EP, CAP, COLS)), struct(...]
  transfers between devices with their start and end apart: 1 -> 0, of which waited for: 0 -> 0; matrix products, arithmetic and copies ran while one was open for 0% -> 0% of each run, Pallas kernels for 71% -> 0%
where the time goes in v2:
time: 103 us; the launch traced here: 101 us
  Pallas kernels  99.1 us (96%)
  local copies, waits for them, and re-layouts  1.57 us (2%)
    pallas_call x1, Pallas kernels, body(): pl.pallas_call(main_kernel, out_shape=(struct((N_EP, CAP, COLS)), struct(...  95.6 us
    pallas_call x1, Pallas kernels, body(): pl.pallas_call(combine_kernel, out_shape=struct((512, COLS)), in_specs=[V...  3.5 us

profile of v2, /device:TPU:1, one launch (start us, length us, event | category | flops | bytes accessed | tf_op | source)
XLA Modules:
  0.0 101.3 jit_solution(11648732044856975744)
XLA Ops:
  0.6 95.6 %exchange.1 = (bf16[64,16,512]{2,1,0:T(8,128)(2,1)}, s32[2,512]{1,0:T(2,128)}, bf16[32,2048]{1,0:T(8,128)(2,1)}) custom-call(f32[1,2048]{1,0:T(1,128)} %bitcast.15, s32[2,512]{1,0:T(2,128)} %bitcast.16, bf16[128,256]{1,0:T(8,128)(2,1)} %klat_ref.1, bf16[64,128]{1,0:T(8,128)(2,1)} %bitcast.14, f32[1,256]{1,0:T(1,128)} %bitcast.19, bf16[128,512]{1,0:T(8,128)(2,1)} %qlat_ref.1, ...), custom_call_target="tpu_custom_call" | custom-call | tf_op jit(solution)/shard_map/exchange/pallas_call | solution.py:484
  96.3 3.5 %combine.1 = bf16[512,512]{1,0:T(8,128)(2,1)} custom-call(s32[2,512]{1,0:T(2,128)} %get-tuple-element.6.target_ref, f32[2,512]{1,0:T(2,128)} %bitcast.17, bf16[1024,512]{1,0:T(8,128)(2,1)} %bitcast.13), custom_call_target="tpu_custom_call" | custom-call | tf_op jit(solution)/shard_map/combine/pallas_call | solution.py:534
  99.8 1.6 %copy.22 = bf16[32,2048]{1,0:T(8,128)(2,1)} copy(bf16[32,2048]{1,0:T(8,128)(2,1)} %get-tuple-element.10) | data formatting | bytes 262144

commit v3 on v2

--- a/solution.py
+++ b/solution.py
@@ -28,7 +28,7 @@
 COLS = 512
 CHUNK = PER_Z * CAP
 HALF = CHUNK // 2
-VMEM_LIMIT = 60 * 1024 * 1024
+VMEM_LIMIT = 62 * 1024 * 1024
 
 
 def rotary_consts():
@@ -75,8 +75,20 @@
 NT = (((1,), (1,)), ((), ()))
 
 
+ORDER_BENDS = ((2, 6), (-2, 5), (1, 4), (-4, 3), (3, 2))
+
+
 def chunk_offset(c):
-    return (c % 2) * (4 + c // 2) + (1 - c % 2) * ((4 - c // 2) % 4)
+    bend = sum(k * ((c + start) // 8) for k, start in ORDER_BENDS)
+    return c + bend
+
+
+def all_columns(c):
+    return c == 0
+
+
+def latent_offset(a):
+    return (a % 2) * ((a + 1) // 2) + (1 - a % 2) * ((8 - a // 2) % 8)
 
 
 def remote(src, dst, send, recv, where):
@@ -86,12 +98,12 @@
 
 
 def main_kernel(
-    gain_ref, route_ref, klat_ref, rope_ref, kgain_ref, qlat_ref, qgain_ref, rows_ref, cols_ref,
+    gain_ref, route_ref, weight_ref, klat_ref, rope_ref, kgain_ref, qlat_ref, qgain_ref, rows_ref, cols_ref,
     tok_hbm, wg_hbm, wu_hbm, wd_hbm, wq_hbm, wqr_hbm, wk_hbm, wv_hbm, wo_hbm,
-    ret_ref, target_ref, mixed_ref,
+    moe_ref, mixed_ref,
     tok, wg, wu, wq, wqr, wk, wv, wo, wdq, relay_p, relay_m,
-    normed, outg, arr, hid, res, lat, query, qrot, top, total, acc, mix, got,
-    wsem, send, rwd, rmix, ra2a, ry0p, ry0m, rfwp, rfwm, rh0p, rh0m, rhfp, rhfm, rret, rlz, rlx, rld,
+    normed, outg, arr, hid, res, ret, columned, lat, query, qrot, top, total, acc, mix, got,
+    wsem, send, rwd, rmix, ra2a, ry0p, ry0m, rfwp, rfwm, rh0p, rh0m, rhfp, rhfm, rret, rlz, rlxp, rlxm, rlfp, rlfm, rld,
 ):
     ep = lax.axis_index("ep")
     tp = lax.axis_index("tp")
@@ -147,8 +159,8 @@
     earlier = jnp.dot((hit0 + hit1).astype(BF16), before.astype(BF16), preferred_element_type=F32)
     slot0 = jnp.sum(hit0 * earlier, axis=0, keepdims=True).astype(jnp.int32)
     slot1 = jnp.sum(hit1 * earlier, axis=0, keepdims=True).astype(jnp.int32)
-    target_ref[0:1, :] = first * CAP + slot0
-    target_ref[1:2, :] = second * CAP + slot1
+    target0 = first * CAP + slot0
+    target1 = second * CAP + slot1
 
     loads[0].wait()
 
@@ -157,17 +169,8 @@
         sel = pl.ds(pl.multiple_of(i * 64, 64), 64)
         wide = tok[sel, :].astype(F32)
         scale = lax.rsqrt(jnp.mean(wide * wide, axis=-1, keepdims=True) + epsilon)
-        part = tok[sel, columns(tp)].astype(F32)
-        normed[sel, :] = (part * scale * gain_ref[:, columns(tp)]).astype(BF16)
-
-    @pl.loop(0, 4)
-    def _(i):
-        ids = lax.broadcasted_iota(jnp.int32, (256, 512), 0) + i * 256
-        pick = ((ids == target_ref[0:1, :]) | (ids == target_ref[1:2, :])).astype(BF16)
-        rows = jnp.dot(pick, normed[...], preferred_element_type=F32).astype(BF16)
-        outg[pl.ds(i * CAP, CAP)] = rows.reshape(CAP, CAP, COLS)
-
-    arr[tp, pl.ds(ep, 1)] = outg[pl.ds(ep, 1)]
+        normed[sel, :] = (wide * scale * gain_ref[...]).astype(BF16)
+
     pl.semaphore_wait(barrier, N_EP - 1 + 3)
 
     def y_copy(src, dst, send_at, recv, where):
@@ -178,26 +181,100 @@
     y_copy(wd_hbm.at[pl.ds(0, 128), columns(across)], relay_p, 2, rwd.at[2], up).start()
     y_copy(wd_hbm.at[pl.ds(128, 128), columns(across)], relay_m, 3, rwd.at[3], down).start()
 
-    @pl.loop(0, N_Z)
-    def _(c):
+    def latent_plane(a):
+        return (z + N_Z - latent_offset(a)) % N_Z
+
+    def ep_at(z_at, x_at):
+        return ((z_at + N_Z) % N_Z) * PER_Z + ((x_at + 4) % 4) * 2 + core
+
+    def latents_x(a):
+        block = lat.at[core, latent_plane(a), x]
+
+        def along_z(step, which):
+            remote(block, block, send.at[7], rlz.at[which], {"ep": ep_at(z + step, x)}).start()
+
+        @pl.when(a != 0)
+        def _():
+            remote(block, block, send.at[7], rlz.at[a], {"tp": up}).wait_recv()
+
+        @pl.when(a == 0)
+        def _():
+            along_z(1, 1)
+            along_z(-1, 2)
+
+        @pl.when((a % 2 == 1) & (a < 7))
+        def _():
+            along_z(1, a + 2)
+
+        @pl.when((a % 2 == 0) & (a > 0) & (a < 6))
+        def _():
+            along_z(-1, a + 2)
+
+        remote(block, block, send.at[17], rlxp.at[a], {"ep": ep_at(z, x + 1)}).start()
+        remote(block, block, send.at[17], rlxm.at[a], {"ep": ep_at(z, x - 1)}).start()
+
+    def latents_on(a):
+        at = latent_plane(a)
+        below = lat.at[core, at, (x + 3) % 4]
+        remote(below, below, send.at[17], rlxp.at[a], {"tp": up}).wait_recv()
+        half = lat.at[core, at, (x + 3) % 4, pl.ds(0, 80)]
+        remote(half, half, send.at[22], rlfp.at[a], {"ep": ep_at(z, x + 1)}).start()
+        above = lat.at[core, at, (x + 1) % 4]
+        remote(above, above, send.at[17], rlxm.at[a], {"tp": up}).wait_recv()
+        half = lat.at[core, at, (x + 1) % 4, pl.ds(80, 80)]
+        remote(half, half, send.at[22], rlfm.at[a], {"ep": ep_at(z, x - 1)}).start()
+
+    def latents_core(a):
+        at = latent_plane(a)
+        half = lat.at[core, at, (x + 2) % 4, pl.ds(0, 80)]
+        remote(half, half, send.at[22], rlfp.at[a], {"tp": up}).wait_recv()
+        half = lat.at[core, at, (x + 2) % 4, pl.ds(80, 80)]
+        remote(half, half, send.at[22], rlfm.at[a], {"tp": up}).wait_recv()
+        four = lat.at[core, at]
+        remote(four, four, send.at[18], rld.at[a], {"ep": z * PER_Z + x * 2 + (1 - core)}).start()
+
+    latents_x(0)
+
+    def rows_out(c):
         zd = (z + chunk_offset(c)) % N_Z
         far = zd * PER_Z
-
-        def put(other):
-            remote(outg.at[other], arr.at[tp, ep], send.at[6], ra2a.at[c], {"ep": other}).start()
-
-        @pl.when(c != 0)
-        def _():
-            put(far + xc)
-
-        @pl.loop(1, PER_Z)
-        def _(j):
-            put(far + (xc + j) % PER_Z)
-
-        @pl.when(c != 0)
-        def _():
-            mine = lat.at[core, z, x]
-            remote(mine, mine, send.at[7], rlz.at[c], {"ep": far + xc}).start()
+        ids = lax.broadcasted_iota(jnp.int32, (CHUNK, 512), 0) + zd * CHUNK
+        pick = ((ids == target0) | (ids == target1)).astype(BF16)
+
+        def take(q):
+            rows = jnp.dot(pick, normed[:, columns(q)], preferred_element_type=F32).astype(BF16)
+            outg[q, pl.ds(far, PER_Z)] = rows.reshape(PER_Z, CAP, COLS)
+
+        @pl.when(all_columns(c))
+        def _():
+            for q in range(N_TP):
+                take(q)
+
+            def put(other):
+                remote(
+                    outg.at[:, other], arr.at[:, ep], send.at[23], ra2a.at[c], {"ep": other}
+                ).start()
+
+            @pl.loop(1, PER_Z)
+            def _(j):
+                put(far + (xc + j) % PER_Z)
+
+        @pl.when(jnp.logical_not(all_columns(c)))
+        def _():
+            take(tp)
+
+            @pl.loop(0, PER_Z)
+            def _(j):
+                other = far + (xc + j) % PER_Z
+                remote(
+                    outg.at[tp, other], arr.at[tp, ep], send.at[6], ra2a.at[c], {"ep": other}
+                ).start()
+
+    @pl.loop(0, N_Z)
+    def _(i):
+        rows_out(i + (7 - i) // 7 - (8 - i) // 7 + (8 - i) // 8)
+
+    arr[:, pl.ds(ep, 1)] = outg[:, pl.ds(ep, 1)]
 
     for load in loads[1:]:
         load.wait()
@@ -219,31 +296,21 @@
     none = jnp.zeros((256, 128), BF16)
     for g, pair in enumerate(((near, none), (far, none), (none, near), (none, far))):
         qrot[g] = jnp.concatenate(pair, axis=1)
+    columned[...] = jnp.concatenate(
+        [target0.astype(F32), target1.astype(F32), weight_ref[...], jnp.zeros((124, 512), F32)], axis=0
+    ).T
+    moe_ref[...] = jnp.zeros((512, COLS), F32)
     top[...] = jnp.full((256, 1), -1e30, F32)
     total[...] = jnp.zeros((256, 1), F32)
     acc[...] = jnp.zeros((256, 256), F32)
 
-    y_copy(relay_p, relay_p, 2, rwd.at[2], up).wait_recv()
-    y_copy(relay_p, wdq.at[down, pl.ds(0, 128)], 4, rwd.at[4], up).start()
-    y_copy(relay_m, relay_m, 3, rwd.at[3], down).wait_recv()
-    y_copy(relay_m, wdq.at[up, pl.ds(128, 128)], 5, rwd.at[5], down).start()
-
     def plane(c):
         return (z + N_Z - chunk_offset(c)) % N_Z
 
     def tokens_in(c):
         at = plane(c) * PER_Z
         whole = arr.at[tp, pl.ds(at, PER_Z)]
-        less = arr.at[tp, pl.ds(0, PER_Z - 1)]
-
-        @pl.when(c == 0)
-        def _():
-            remote(less, less, send.at[6], ra2a.at[c], {"tp": up}).wait_recv()
-
-        @pl.when(c != 0)
-        def _():
-            remote(whole, whole, send.at[6], ra2a.at[c], {"tp": up}).wait_recv()
-
+        remote(whole, whole, send.at[6], ra2a.at[c], {"tp": up}).wait_recv()
         y_copy(whole, whole, 8, ry0p.at[c], up).start()
         y_copy(whole, whole, 9, ry0m.at[c], down).start()
 
@@ -260,10 +327,19 @@
 
     def hidden_units(c):
         at = plane(c) * PER_Z
-        half = arr.at[across, pl.ds(at, PER_Z // 2)]
-        y_copy(half, half, 10, rfwp.at[c], up).wait_recv()
-        half = arr.at[across, pl.ds(at + PER_Z // 2, PER_Z // 2)]
-        y_copy(half, half, 11, rfwm.at[c], down).wait_recv()
+
+        @pl.when(c == 0)
+        def _():
+            less = arr.at[:, pl.ds(0, PER_Z - 1)]
+            remote(less, less, send.at[23], ra2a.at[c], {"tp": up}).wait_recv()
+
+        @pl.when(jnp.logical_not(all_columns(c)))
+        def _():
+            half = arr.at[across, pl.ds(at, PER_Z // 2)]
+            y_copy(half, half, 10, rfwp.at[c], up).wait_recv()
+            half = arr.at[across, pl.ds(at + PER_Z // 2, PER_Z // 2)]
+            y_copy(half, half, 11, rfwm.at[c], down).wait_recv()
+
         gate = jnp.zeros((CHUNK, 256), F32)
         upper = jnp.zeros((CHUNK, 256), F32)
         for q in range(N_TP):
@@ -307,7 +383,7 @@
 
         def put(j):
             remote(
-                res.at[c, j], ret_ref.at[ep], send.at[16], rret.at[c], {"ep": at + j}
+                res.at[c, j], ret.at[ep], send.at[16], rret.at[c], {"ep": at + j}
             ).start()
 
         @pl.when(c != 0)
@@ -316,32 +392,45 @@
 
         @pl.when(c == 0)
         def _():
-            ret_ref[pl.ds(ep, 1)] = res[c, pl.ds(xc, 1)]
+            ret[pl.ds(ep, 1)] = res[c, pl.ds(xc, 1)]
 
         @pl.loop(1, PER_Z)
         def _(j):
             put((xc + j) % PER_Z)
 
-    def latents_x(c):
-        block = lat.at[core, plane(c), x]
+    def combine(c):
+        far = ((z + chunk_offset(c)) % N_Z) * PER_Z
+        whole = ret.at[pl.ds(far, PER_Z)]
+        less = ret.at[pl.ds(0, PER_Z - 1)]
+
+        @pl.when(c == 0)
+        def _():
+            remote(less, less, send.at[16], rret.at[c], {"tp": up}).wait_recv()
 
         @pl.when(c != 0)
         def _():
-            remote(block, block, send.at[7], rlz.at[c], {"tp": up}).wait_recv()
-
-        @pl.loop(1, 4)
-        def _(j):
-            there = z * PER_Z + ((x + j) % 4) * 2 + core
-            remote(block, block, send.at[17], rlx.at[c], {"ep": there}).start()
-
-    def latents_core(c):
-        three = lat.at[core, 0, pl.ds(0, 3)]
-        remote(three, three, send.at[17], rlx.at[c], {"tp": up}).wait_recv()
-        four = lat.at[core, plane(c)]
-        remote(four, four, send.at[18], rld.at[c], {"ep": z * PER_Z + x * 2 + (1 - core)}).start()
+            remote(whole, whole, send.at[16], rret.at[c], {"tp": up}).wait_recv()
+
+        ids = (lax.broadcasted_iota(jnp.int32, (128, CHUNK), 1) + far * CAP).astype(F32)
+        back = ret[pl.ds(far, PER_Z)].reshape(CHUNK, COLS)
+
+        for i in range(4):
+            sel = slice(i * 128, (i + 1) * 128)
+            sums = moe_ref[sel, :]
+            for k in range(2):
+                pick = (ids == columned[sel, k : k + 1]).astype(BF16)
+                got_rows = jnp.dot(pick, back, preferred_element_type=F32)
+                sums += got_rows * columned[sel, 2 + k : 3 + k]
+            moe_ref[sel, :] = sums
+
+    def relay(c):
+        y_copy(relay_p, relay_p, 2, rwd.at[2], up).wait_recv()
+        y_copy(relay_p, wdq.at[down, pl.ds(0, 128)], 4, rwd.at[4], up).start()
+        y_copy(relay_m, relay_m, 3, rwd.at[3], down).wait_recv()
+        y_copy(relay_m, wdq.at[up, pl.ds(128, 128)], 5, rwd.at[5], down).start()
 
     def attend(c):
-        at = plane(c)
+        at = latent_plane(c)
         four = lat.at[1 - core, at]
         remote(four, four, send.at[18], rld.at[c], {"tp": up}).wait_recv()
         turned = lat[:, at, :, 128:160, :].reshape(256, 256)
@@ -387,19 +476,41 @@
         for i in range(1, N_TP):
             mix_copy(i).start()
 
+    def twice(stage, start):
+        def both(c):
+            stage(start + 2 * c)
+            stage(start + 1 + 2 * c)
+
+        both.__name__ = stage.__name__
+        return both
+
+    def after(stage, start):
+        def later(c):
+            stage(start + c)
+
+        later.__name__ = stage.__name__
+        return later
+
     plan = (
-        (0, N_Z, tokens_in),
-        (0, N_Z, latents_x),
-        (1, N_Z, tokens_on),
-        (1, N_Z, latents_core),
-        (2, N_Z, hidden_units),
-        (2, N_Z, attend),
-        (3, N_Z, hidden_on),
-        (4, N_Z, results_out),
-        (10, 1, project),
+        (0, 7, after(tokens_in, 1)),
+        (0, 1, relay),
+        (1, 7, after(tokens_on, 1)),
+        (1, 8, hidden_units),
+        (2, 8, hidden_on),
+        (3, 8, results_out),
+        (0, 3, after(latents_x, 1)),
+        (3, 2, twice(latents_x, 4)),
+        (0, 4, latents_on),
+        (4, 2, twice(latents_on, 4)),
+        (1, 4, latents_core),
+        (5, 2, twice(latents_core, 4)),
+        (2, 4, attend),
+        (6, 2, twice(attend, 4)),
+        (9, 1, project),
+        (6, N_Z, combine),
     )
 
-    @pl.loop(0, 12)
+    @pl.loop(0, 14)
     def _(i):
         for lag, count, stage in plan:
 
@@ -411,21 +522,7 @@
     for i in range(1, N_TP):
         mix_copy(i).wait()
         sums = sums + got[i].astype(F32)
-    mixed_ref[...] = sums.astype(BF16)
-
-    @pl.loop(0, N_Z)
-    def _(c):
-        far = ((z + chunk_offset(c)) % N_Z) * PER_Z
-        whole = ret_ref.at[pl.ds(far, PER_Z)]
-        less = ret_ref.at[pl.ds(0, PER_Z - 1)]
-
-        @pl.when(c == 0)
-        def _():
-            remote(less, less, send.at[16], rret.at[c], {"tp": up}).wait_recv()
-
-        @pl.when(c != 0)
-        def _():
-            remote(whole, whole, send.at[16], rret.at[c], {"tp": up}).wait_recv()
+    mixed_ref[...] = sums
 
     def sent(ref, which):
         remote(ref, ref, send.at[which], ra2a.at[0], {"tp": up}).wait_send()
@@ -434,34 +531,26 @@
         sent(wdq.at[0], which)
     for which in (2, 3, 4, 5):
         sent(relay_p, which)
-    sent(outg.at[pl.ds(0, N_EP - 1)], 6)
+    sent(outg.at[0, pl.ds(0, 56)], 6)
+    sent(outg.at[:, pl.ds(0, 7)], 23)
     sent(lat.at[0, pl.ds(0, 7), 0], 7)
     for which in (8, 9):
-        sent(arr.at[0], which)
+        sent(arr.at[0, pl.ds(0, 56)], which)
     for which in (10, 11):
-        sent(arr.at[0, pl.ds(0, N_EP // 2)], which)
+        sent(arr.at[0, pl.ds(0, 28)], which)
     for which in (12, 13):
         sent(hid.at[:, 0], which)
     for which in (14, 15):
         sent(hid.at[:, 0, pl.ds(0, HALF)], which)
-    sent(outg.at[pl.ds(0, N_EP - 1)], 16)
-    sent(lat.at[0, :, pl.ds(0, 3)], 17)
+    sent(ret.at[pl.ds(0, N_EP - 1)], 16)
+    sent(lat.at[0, :, pl.ds(0, 2)], 17)
+    sent(lat.at[0, :, 0], 22)
     sent(lat.at[0], 18)
 
 
-def combine_kernel(target_ref, weight_ref, ret_ref, out_ref):
-    pad = jnp.zeros((124, 512), F32)
-    both = jnp.concatenate([target_ref[...].astype(F32), weight_ref[...], pad], axis=0)
-    turned = both.T
-    for i in range(4):
-        rows = turned[i * 128 : (i + 1) * 128]
-        ids = lax.broadcasted_iota(jnp.int32, (128, 1024), 1)
-        total = jnp.zeros((128, COLS), F32)
-        for c in range(2):
-            pick = (ids == rows[:, c : c + 1].astype(jnp.int32)).astype(BF16)
-            got = jnp.dot(pick, ret_ref[...], preferred_element_type=F32)
-            total = total + got * rows[:, 2 + c : 3 + c]
-        out_ref[i * 128 : (i + 1) * 128, :] = total.astype(BF16)
+def finish_kernel(moe_ref, mixed_ref, moe_out, mixed_out):
+    moe_out[...] = moe_ref[...].astype(BF16)
+    mixed_out[...] = mixed_ref[...].astype(BF16)
 
 
 VM = pl.BlockSpec(memory_space=pltpu.VMEM)
@@ -481,15 +570,14 @@
     cols = jnp.asarray(cols_np)
     dma = pltpu.SemaphoreType.DMA
 
-    returned, target, mixer_out = pl.pallas_call(
+    moe, mixed = pl.pallas_call(
         main_kernel,
         out_shape=(
-            struct((N_EP, CAP, COLS)),
-            struct((2, 512), jnp.int32),
-            struct((32, 2048)),
+            struct((512, COLS), F32),
+            struct((32, 2048), F32),
         ),
-        in_specs=[VM] * 9 + [ANY] * 9,
-        out_specs=(VM, VM, VM),
+        in_specs=[VM] * 10 + [ANY] * 9,
+        out_specs=(VM, VM),
         scratch_shapes=[
             pltpu.VMEM(shape, dtype)
             for shape, dtype in (
@@ -504,11 +592,13 @@
                 ((N_TP, 256, COLS), BF16),
                 ((128, COLS), BF16),
                 ((128, COLS), BF16),
-                ((512, COLS), BF16),
-                ((N_EP, CAP, COLS), BF16),
+                ((512, 2048), BF16),
+                ((N_TP, N_EP, CAP, COLS), BF16),
                 ((N_TP, N_EP, CAP, COLS), BF16),
                 ((N_Z, N_TP, CHUNK, 256), BF16),
                 ((N_Z, PER_Z, CAP, COLS), BF16),
+                ((N_EP, CAP, COLS), BF16),
+                ((512, 128), F32),
                 ((2, N_Z, 4, 160, 256), BF16),
                 ((256, 256), BF16),
                 ((4, 256, 256), BF16),
@@ -519,26 +609,26 @@
                 ((N_TP, 32, 2048), BF16),
             )
         ]
-        + [dma((9,)), dma((22,)), dma((6,)), dma((N_TP,))]
-        + [dma((N_Z,))] * 13,
+        + [dma((9,)), dma((24,)), dma((6,)), dma((N_TP,))]
+        + [dma((N_Z,))] * 16,
         compiler_params=pltpu.CompilerParams(
             collective_id=0, has_side_effects=True, vmem_limit_bytes=VMEM_LIMIT
         ),
         name="exchange",
     )(
-        ffn_gain.reshape(1, -1), route_expert.T, key_latent, rope_key.T, key_gain.reshape(1, -1),
+        ffn_gain.reshape(1, -1), route_expert.T, route_weight.T, key_latent, rope_key.T, key_gain.reshape(1, -1),
         query_latent, query_gain.reshape(1, -1), rows, cols,
         tokens_b, w_gate[0], w_up[0], w_down[0], w_query, w_query_rope, w_key, w_value, w_out,
     )
 
-    moe_out = pl.pallas_call(
-        combine_kernel,
-        out_shape=struct((512, COLS)),
-        in_specs=[VM] * 3,
-        out_specs=VM,
+    moe_out, mixer_out = pl.pallas_call(
+        finish_kernel,
+        out_shape=(struct((512, COLS)), struct((32, 2048))),
+        in_specs=[VM] * 2,
+        out_specs=(VM, VM),
         compiler_params=pltpu.CompilerParams(vmem_limit_bytes=VMEM_LIMIT),
-        name="combine",
-    )(target, route_weight.T, returned.reshape(N_EP * CAP, COLS))
+        name="finish",
+    )(moe, mixed)
 
     return (mixer_out, moe_out)
 

time: 103 us -> 98.2 us (0.953); the launches traced: 101 us -> 98.1 us
  Pallas kernels: 99.1 us -> 97.4 us
  local copies, waits for them, and re-layouts: 1.57 us -> 0 us
    pallas_call x2, Pallas kernels: 99.1 us -> 97.4 us  [the longest x1 95.3 us: body(): pl.pallas_call(main_kernel, out_shape=(struct((512, COLS), F32), struct((...]
    unnamed x1 -> x0, local copies, waits for them, and re-layouts: 1.57 us -> none
where the time goes in v3:
time: 98.2 us; the launch traced here: 98.1 us
  Pallas kernels  97.4 us (99%)
    pallas_call x1, Pallas kernels, body(): pl.pallas_call(main_kernel, out_shape=(struct((512, COLS), F32), struct((...  95.3 us
    pallas_call x1, Pallas kernels, body(): pl.pallas_call(finish_kernel, out_shape=(struct((512, COLS)), struct((32,...  2.15 us

profile of v3, /device:TPU:1, one launch (start us, length us, event | category | flops | bytes accessed | tf_op | source)
XLA Modules:
  0.0 98.1 jit_solution(5528717426156830463)
XLA Ops:
  0.6 95.3 %exchange.1 = (f32[512,512]{1,0:T(8,128)}, f32[32,2048]{1,0:T(8,128)}) custom-call(f32[1,2048]{1,0:T(1,128)} %bitcast.13, s32[2,512]{1,0:T(2,128)} %bitcast.14, f32[2,512]{1,0:T(2,128)} %bitcast.15, bf16[128,256]{1,0:T(8,128)(2,1)} %klat_ref.1, bf16[64,128]{1,0:T(8,128)(2,1)} %bitcast.12, f32[1,256]{1,0:T(1,128)} %bitcast.17, bf16[128,512]{1,0:T(8,128)(2,1)} %qlat_ref.1, ...), custom_call_target="tpu_custom_call" | custom-call | tf_op jit(solution)/shard_map/exchange/pallas_call | solution.py:573
  95.9 2.1 %finish.1 = (bf16[512,512]{1,0:T(8,128)(2,1)}, bf16[32,2048]{1,0:T(8,128)(2,1)}) custom-call(f32[512,512]{1,0:T(8,128)} %get-tuple-element.6.moe_ref, f32[32,2048]{1,0:T(8,128)} %get-tuple-element.7.mixed_ref), custom_call_target="tpu_custom_call" | custom-call | tf_op jit(solution)/shard_map/finish/pallas_call | solution.py:624

commit v4 on v3

--- a/solution.py
+++ b/solution.py
@@ -53,8 +53,8 @@
     return rows, cols
 
 
-def cos_sin(rows_ref, cols_ref, ep):
-    rows = rows_ref[ep]
+def cos_sin(rows_ref, cols_ref):
+    rows = rows_ref[...]
     cos = jnp.concatenate([rows[0:1] + cols_ref[0], rows[1:2] + cols_ref[0]], axis=0)
     sin = jnp.concatenate([rows[2:3] + cols_ref[1], rows[3:4] + cols_ref[1]], axis=0)
     return cos, sin
@@ -75,7 +75,7 @@
 NT = (((1,), (1,)), ((), ()))
 
 
-ORDER_BENDS = ((2, 6), (-2, 5), (1, 4), (-4, 3), (3, 2))
+ORDER_BENDS = ((1, 7), (2, 6), (-3, 5), (1, 3), (-6, 2), (5, 1))
 
 
 def chunk_offset(c):
@@ -98,9 +98,10 @@
 
 
 def main_kernel(
-    gain_ref, route_ref, weight_ref, klat_ref, rope_ref, kgain_ref, qlat_ref, qgain_ref, rows_ref, cols_ref,
+    gain_hbm, route_hbm, weight_hbm, klat_hbm, rope_hbm, kgain_hbm, qlat_hbm, qgain_hbm, rows_hbm, cols_hbm,
     tok_hbm, wg_hbm, wu_hbm, wd_hbm, wq_hbm, wqr_hbm, wk_hbm, wv_hbm, wo_hbm,
     moe_ref, mixed_ref,
+    gain_ref, route_ref, weight_ref, klat_ref, rope_ref, kgain_ref, qlat_ref, qgain_ref, rows_ref, cols_ref,
     tok, wg, wu, wq, wqr, wk, wv, wo, wdq, relay_p, relay_m,
     normed, outg, arr, hid, res, ret, columned, lat, query, qrot, top, total, acc, mix, got,
     wsem, send, rwd, rmix, ra2a, ry0p, ry0m, rfwp, rfwm, rh0p, rh0m, rhfp, rhfm, rret, rlz, rlxp, rlxm, rlfp, rlfm, rld,
@@ -130,14 +131,20 @@
         return pl.ds(pl.multiple_of(which * COLS, COLS), COLS)
 
     pairs = (
-        (tok_hbm, tok), (wd_hbm.at[:, columns(tp)], wdq.at[tp]), (wg_hbm, wg), (wu_hbm, wu),
+        (klat_hbm, klat_ref), (kgain_hbm, kgain_ref), (rope_hbm, rope_ref),
+        (rows_hbm.at[ep], rows_ref), (cols_hbm, cols_ref), (route_hbm, route_ref),
+        (gain_hbm, gain_ref), (tok_hbm, tok), (weight_hbm, weight_ref), (qlat_hbm, qlat_ref),
+        (qgain_hbm, qgain_ref), (wd_hbm.at[:, columns(tp)], wdq.at[tp]), (wg_hbm, wg), (wu_hbm, wu),
         (wq_hbm, wq), (wqr_hbm, wqr), (wk_hbm, wk), (wv_hbm, wv), (wo_hbm, wo),
     )
     loads = [pltpu.make_async_copy(src, dst, wsem.at[i]) for i, (src, dst) in enumerate(pairs)]
     for load in loads:
         load.start()
 
-    cos, sin = cos_sin(rows_ref, cols_ref, ep)
+    for load in loads[0:6]:
+        load.wait()
+
+    cos, sin = cos_sin(rows_ref, cols_ref)
     lat[core, z, x, 0:128, :] = rms(klat_ref[...], kgain_ref[...])
     rope = rope_ref[...].astype(F32)
     rope = jnp.concatenate([rope, rope], axis=0).T
@@ -162,15 +169,6 @@
     target0 = first * CAP + slot0
     target1 = second * CAP + slot1
 
-    loads[0].wait()
-
-    @pl.loop(0, 8)
-    def _(i):
-        sel = pl.ds(pl.multiple_of(i * 64, 64), 64)
-        wide = tok[sel, :].astype(F32)
-        scale = lax.rsqrt(jnp.mean(wide * wide, axis=-1, keepdims=True) + epsilon)
-        normed[sel, :] = (wide * scale * gain_ref[...]).astype(BF16)
-
     pl.semaphore_wait(barrier, N_EP - 1 + 3)
 
     def y_copy(src, dst, send_at, recv, where):
@@ -235,6 +233,16 @@
 
     latents_x(0)
 
+    loads[6].wait()
+    loads[7].wait()
+
+    @pl.loop(0, 8)
+    def _(i):
+        sel = pl.ds(pl.multiple_of(i * 64, 64), 64)
+        wide = tok[sel, :].astype(F32)
+        scale = lax.rsqrt(jnp.mean(wide * wide, axis=-1, keepdims=True) + epsilon)
+        normed[sel, :] = (wide * scale * gain_ref[...]).astype(BF16)
+
     def rows_out(c):
         zd = (z + chunk_offset(c)) % N_Z
         far = zd * PER_Z
@@ -276,7 +284,7 @@
 
     arr[:, pl.ds(ep, 1)] = outg[:, pl.ds(ep, 1)]
 
-    for load in loads[1:]:
+    for load in loads[8:]:
         load.wait()
 
     qn = rms(qlat_ref[...], qgain_ref[...])
@@ -498,19 +506,24 @@
         (1, 8, hidden_units),
         (2, 8, hidden_on),
         (3, 8, results_out),
-        (0, 3, after(latents_x, 1)),
-        (3, 2, twice(latents_x, 4)),
-        (0, 4, latents_on),
-        (4, 2, twice(latents_on, 4)),
-        (1, 4, latents_core),
-        (5, 2, twice(latents_core, 4)),
-        (2, 4, attend),
-        (6, 2, twice(attend, 4)),
+        (0, 2, after(latents_x, 1)),
+        (3, 2, twice(latents_x, 3)),
+        (5, 1, after(latents_x, 7)),
+        (0, 3, latents_on),
+        (4, 2, twice(latents_on, 3)),
+        (6, 1, after(latents_on, 7)),
+        (1, 3, latents_core),
+        (5, 2, twice(latents_core, 3)),
+        (7, 1, after(latents_core, 7)),
+        (2, 3, attend),
+        (6, 2, twice(attend, 3)),
+        (9, 1, after(attend, 7)),
         (9, 1, project),
-        (6, N_Z, combine),
+        (6, 2, combine),
+        (10, 6, after(combine, 2)),
     )
 
-    @pl.loop(0, 14)
+    @pl.loop(0, 16)
     def _(i):
         for lag, count, stage in plan:
 
@@ -576,11 +589,21 @@
             struct((512, COLS), F32),
             struct((32, 2048), F32),
         ),
-        in_specs=[VM] * 10 + [ANY] * 9,
+        in_specs=[ANY] * 19,
         out_specs=(VM, VM),
         scratch_shapes=[
             pltpu.VMEM(shape, dtype)
             for shape, dtype in (
+                ((1, 2048), F32),
+                ((2, 512), jnp.int32),
+                ((2, 512), F32),
+                ((128, 256), BF16),
+                ((64, 128), BF16),
+                ((1, 256), F32),
+                ((128, 512), BF16),
+                ((1, 512), F32),
+                ((4, 128), F32),
+                ((2, 64, 128), F32),
                 ((512, 2048), BF16),
                 ((2048, 256), BF16),
                 ((2048, 256), BF16),
@@ -609,7 +632,7 @@
                 ((N_TP, 32, 2048), BF16),
             )
         ]
-        + [dma((9,)), dma((24,)), dma((6,)), dma((N_TP,))]
+        + [dma((19,)), dma((24,)), dma((6,)), dma((N_TP,))]
         + [dma((N_Z,))] * 16,
         compiler_params=pltpu.CompilerParams(
             collective_id=0, has_side_effects=True, vmem_limit_bytes=VMEM_LIMIT

time: 98.2 us -> 91.9 us (0.936)
  Pallas kernels: 97.4 us -> 91.2 us
    pallas_call x1, Pallas kernels: 95.3 us -> 89.1 us  [body(): pl.pallas_call(main_kernel, out_shape=(struct((512, COLS), F32), struct((...]
where the time goes in v4:
time: 91.9 us; the launch traced here: 91.8 us
  Pallas kernels  91.2 us (99%)
    pallas_call x1, Pallas kernels, body(): pl.pallas_call(main_kernel, out_shape=(struct((512, COLS), F32), struct((...  89.1 us
    pallas_call x1, Pallas kernels, body(): pl.pallas_call(finish_kernel, out_shape=(struct((512, COLS)), struct((32,...  2.15 us

profile of v4, /device:TPU:1, one launch (start us, length us, event | category | flops | bytes accessed | tf_op | source)
XLA Modules:
  0.0 91.8 jit_solution(11131005478056499252)
XLA Ops:
  0.6 89.1 %exchange.1 = (f32[512,512]{1,0:T(8,128)}, f32[32,2048]{1,0:T(8,128)}) custom-call(f32[1,2048]{1,0:T(1,128)} %bitcast.13, s32[2,512]{1,0:T(2,128)} %bitcast.14, f32[2,512]{1,0:T(2,128)} %bitcast.15, bf16[128,256]{1,0:T(8,128)(2,1)} %klat_hbm.1, bf16[64,128]{1,0:T(8,128)(2,1)} %bitcast.12, f32[1,256]{1,0:T(1,128)} %bitcast.17, bf16[128,512]{1,0:T(8,128)(2,1)} %qlat_hbm.1, ...), custom_call_target="tpu_custom_call" | custom-call | tf_op jit(solution)/shard_map/exchange/pallas_call | solution.py:586
  89.7 2.1 %finish.1 = (bf16[512,512]{1,0:T(8,128)(2,1)}, bf16[32,2048]{1,0:T(8,128)(2,1)}) custom-call(f32[512,512]{1,0:T(8,128)} %get-tuple-element.6.moe_ref, f32[32,2048]{1,0:T(8,128)} %get-tuple-element.7.mixed_ref), custom_call_target="tpu_custom_call" | custom-call | tf_op jit(solution)/shard_map/finish/pallas_call | solution.py:647

commit v5 on v4

--- a/solution.py
+++ b/solution.py
@@ -103,7 +103,7 @@
     moe_ref, mixed_ref,
     gain_ref, route_ref, weight_ref, klat_ref, rope_ref, kgain_ref, qlat_ref, qgain_ref, rows_ref, cols_ref,
     tok, wg, wu, wq, wqr, wk, wv, wo, wdq, relay_p, relay_m,
-    normed, outg, arr, hid, res, ret, columned, lat, query, qrot, top, total, acc, mix, got,
+    normed, outg, arr, hid, res, ret, columned, weighed_rows, lat, query, qrot, top, total, acc, mix, got,
     wsem, send, rwd, rmix, ra2a, ry0p, ry0m, rfwp, rfwm, rh0p, rh0m, rhfp, rhfm, rret, rlz, rlxp, rlxm, rlfp, rlfm, rld,
 ):
     ep = lax.axis_index("ep")
@@ -307,7 +307,7 @@
     columned[...] = jnp.concatenate(
         [target0.astype(F32), target1.astype(F32), weight_ref[...], jnp.zeros((124, 512), F32)], axis=0
     ).T
-    moe_ref[...] = jnp.zeros((512, COLS), F32)
+    weighed_rows[...] = jnp.zeros((512, COLS), F32)
     top[...] = jnp.full((256, 1), -1e30, F32)
     total[...] = jnp.zeros((256, 1), F32)
     acc[...] = jnp.zeros((256, 256), F32)
@@ -424,12 +424,12 @@
 
         for i in range(4):
             sel = slice(i * 128, (i + 1) * 128)
-            sums = moe_ref[sel, :]
+            sums = weighed_rows[sel, :]
             for k in range(2):
                 pick = (ids == columned[sel, k : k + 1]).astype(BF16)
                 got_rows = jnp.dot(pick, back, preferred_element_type=F32)
                 sums += got_rows * columned[sel, 2 + k : 3 + k]
-            moe_ref[sel, :] = sums
+            weighed_rows[sel, :] = sums
 
     def relay(c):
         y_copy(relay_p, relay_p, 2, rwd.at[2], up).wait_recv()
@@ -535,7 +535,9 @@
     for i in range(1, N_TP):
         mix_copy(i).wait()
         sums = sums + got[i].astype(F32)
-    mixed_ref[...] = sums
+    mixed_ref[...] = sums.astype(BF16)
+
+    moe_ref[...] = weighed_rows[...].astype(BF16)
 
     def sent(ref, which):
         remote(ref, ref, send.at[which], ra2a.at[0], {"tp": up}).wait_send()
@@ -562,8 +564,8 @@
 
 
 def finish_kernel(moe_ref, mixed_ref, moe_out, mixed_out):
-    moe_out[...] = moe_ref[...].astype(BF16)
-    mixed_out[...] = mixed_ref[...].astype(BF16)
+    moe_out[...] = moe_ref[...]
+    mixed_out[...] = mixed_ref[...]
 
 
 VM = pl.BlockSpec(memory_space=pltpu.VMEM)
@@ -586,8 +588,8 @@
     moe, mixed = pl.pallas_call(
         main_kernel,
         out_shape=(
-            struct((512, COLS), F32),
-            struct((32, 2048), F32),
+            struct((512, COLS)),
+            struct((32, 2048)),
         ),
         in_specs=[ANY] * 19,
         out_specs=(VM, VM),
@@ -622,6 +624,7 @@
                 ((N_Z, PER_Z, CAP, COLS), BF16),
                 ((N_EP, CAP, COLS), BF16),
                 ((512, 128), F32),
+                ((512, COLS), F32),
                 ((2, N_Z, 4, 160, 256), BF16),
                 ((256, 256), BF16),
                 ((4, 256, 256), BF16),

time: 91.9 us -> 91.5 us (level)
  no operation moved by 1% of the time
where the time goes in v5:
time: 91.5 us; the launch traced here: 91.4 us
  Pallas kernels  90.8 us (99%)
    pallas_call x1, Pallas kernels, body(): pl.pallas_call(main_kernel, out_shape=(struct((512, COLS)), struct((32, 2...  88.9 us
    pallas_call x1, Pallas kernels, body(): pl.pallas_call(finish_kernel, out_shape=(struct((512, COLS)), struct((32,...  1.93 us

profile of v5, /device:TPU:1, one launch (start us, length us, event | category | flops | bytes accessed | tf_op | source)
XLA Modules:
  0.0 91.4 jit_solution(10109201038121086874)
XLA Ops:
  0.6 88.9 %exchange.1 = (bf16[512,512]{1,0:T(8,128)(2,1)}, bf16[32,2048]{1,0:T(8,128)(2,1)}) custom-call(f32[1,2048]{1,0:T(1,128)} %bitcast.13, s32[2,512]{1,0:T(2,128)} %bitcast.14, f32[2,512]{1,0:T(2,128)} %bitcast.15, bf16[128,256]{1,0:T(8,128)(2,1)} %klat_hbm.1, bf16[64,128]{1,0:T(8,128)(2,1)} %bitcast.12, f32[1,256]{1,0:T(1,128)} %bitcast.17, ...), custom_call_target="tpu_custom_call" | custom-call | tf_op jit(solution)/shard_map/exchange/pallas_call | solution.py:588
  89.5 1.9 %finish.1 = (bf16[512,512]{1,0:T(8,128)(2,1)}, bf16[32,2048]{1,0:T(8,128)(2,1)}) custom-call(bf16[512,512]{1,0:T(8,128)(2,1)} %get-tuple-element.6.moe_ref, bf16[32,2048]{1,0:T(8,128)(2,1)} %get-tuple-element.7.mixed_ref), custom_call_target="tpu_custom_call" | custom-call | tf_op jit(solution)/shard_map/finish/pallas_call | solution.py:650
